TPU v7x, 32 devices: a whole 2x2x4 slice. The times are simulated.
32 devices in a mesh: fs: 8 (over z, y), tp: 4 (over x, core).
Axes of the slice: x: 2, y: 2, z: 4, core: 2. Of those that a mesh axis runs over, the one named last changes fastest.
Arguments:
- tokens: bfloat16 [2048, 2048], P('fs', 'tp'), may hold values from -12.1 to 12.1, as said below
- gate_weight: float32 [2048, 5632], P('fs', 'tp'), may hold values from -0.125 to 0.125
- up_weight: float32 [2048, 5632], P('fs', 'tp'), may hold values from -0.125 to 0.125
- down_weight: float32 [5632, 2048], P('tp', 'fs'), may hold values from -0.078125 to 0.078125
- gate_scale: float32 [4, 1408], P('tp', 'fs'), may hold values from 0.1 to 1.9
- up_scale: float32 [4, 1408], P('tp', 'fs'), may hold values from 0.1 to 1.9
- down_scale: float32 [4, 512], P('tp', 'fs'), may hold values from 0.16 to 4.6, as said below
- bgate_weight: float32 [2048, 2048], P('fs', 'tp'), may hold values from -0.125 to 0.125
- cgate_weight: float32 [2048, 2048], P('fs', 'tp'), may hold values from -0.125 to 0.125
- value_weight: float32 [2048, 2048], P('fs', 'tp'), may hold values from -0.125 to 0.125
- bgate_scale: float32 [4, 512], P('tp', 'fs'), may hold values from 0.1 to 1.9
- cgate_scale: float32 [4, 512], P('tp', 'fs'), may hold values from 0.1 to 1.9
- value_scale: float32 [4, 512], P('tp', 'fs'), may hold values from 0.1 to 1.9
- conv_taps: float32 [3, 2048], replicated, may hold values from -3.5 to 3.5
- mixout_weight: float32 [2048, 2048], P('tp', 'fs'), may hold values from -0.125 to 0.125
- mixout_scale: float32 [4, 512], P('tp', 'fs'), may hold values from 0.16 to 4.6, as said below
- first_gain: float32 [2048], replicated, may hold values from 0.1 to 1.9
- first_shift: float32 [2048], replicated, may hold values from -1.8 to 1.8
- mixer_gain: float32 [2048], replicated, may hold values from 0.1 to 1.9
- mixer_shift: float32 [2048], replicated, may hold values from -1.8 to 1.8
- last_gain: float32 [2048], replicated, may hold values from 0.1 to 1.9
- last_shift: float32 [2048], replicated, may hold values from -1.8 to 1.8
Outputs:
- layer_out: bfloat16 [2048, 2048], P('fs', 'tp')
Inputs may be any that keep to these rules, and one draw needn't show every extreme that they name: `tokens`: normal values times one factor for each of 4 equal consecutive blocks of the features. `down_scale`: positive; one factor for each row times a spread over the columns. `mixout_scale`: positive; one factor for each row times a spread over the columns.
All inputs are finite; a program needn't handle non-finite values.
Results may differ from a plain program's by a relative error of at most 0.025.
Values may be sent and summed in bfloat16 or wider, within the bound.
A program may use at most 64 MiB of HBM per device.

v0:
```python
import functools

import jax
import jax.numpy as jnp
from jax import lax
from jax.experimental import pallas as pl
from jax.experimental.pallas import tpu as pltpu
from jax.sharding import Mesh
from jax.sharding import PartitionSpec as P

TAPS = 3
LENGTH = 128
CORES = 2

RESIDUAL_SCALE = 1.4142135623730951
HALF_STEP = 0.5
EPSILON = 1e-05
BY_AXIS = pl.DeviceIdType.MESH
ANY = pl.BlockSpec(memory_space=pl.ANY)
VMEM = pl.BlockSpec(memory_space=pltpu.VMEM)


def greet(depth, axes, others=()):
    barrier = pltpu.get_barrier_semaphore()
    z = lax.axis_index("z")
    targets = [{"z": lax.rem(z + d, depth)} for d in range(1, depth)]
    targets += [{axis: 1 - lax.axis_index(axis)} for axis in axes]
    targets += others
    for target in targets:
        pl.semaphore_signal(barrier, inc=1, device_id=target, device_id_type=BY_AXIS)
    pl.semaphore_wait(barrier, len(targets))


def remote(src, dst, send, recv, target):
    return pltpu.make_async_remote_copy(
        src_ref=src, dst_ref=dst, send_sem=send, recv_sem=recv, device_id=target, device_id_type=BY_AXIS
    )


def block_place(ref, px, pz, py, width):
    start = pl.multiple_of((pz * 2 + py) * width, width)
    return ref.at[:, px, :, pl.ds(start, width)]


def weights_kernel(
    depth, w_ref, m_ref, s_ref, t_ref, g_ref, held_ref, sa_ref, ta_ref,
    zsend, zrecv, ysend, yrecv, xsend, xrecv, dsend, drecv, msend, mrecv,
    ssend, srecv, tzsend, tzrecv, tcsend, tcrecv, local,
):
    z, y, x, c = (lax.axis_index(axis) for axis in ("z", "y", "x", "c"))
    width = w_ref.shape[-1]
    greet(depth, ("y", "x", "c"))

    mats = w_ref.shape[1]

    def place(px, pz, py, piece=slice(None)):
        start = pl.multiple_of((pz * 2 + py) * width, width)
        return g_ref.at[piece, px, :, pl.ds(start, width)]

    to_x, to_y, to_c = {"x": 1 - x}, {"y": 1 - y}, {"c": 1 - c}
    scale_sends, token_sends, z_copies, m_copies = [], [], [], []
    keeps = [
        pltpu.make_async_copy(s_ref, sa_ref.at[c, x, y, z], local.at[0]),
        pltpu.make_async_copy(t_ref, ta_ref.at[0, c], local.at[1]),
        pltpu.make_async_copy(w_ref.at[z], place(x, z, y), local.at[2]),
        pltpu.make_async_copy(m_ref.at[z], held_ref.at[0], local.at[3]),
    ]
    for copy in keeps:
        copy.start()
    beside = [remote(t_ref, ta_ref.at[0, c], tcsend.at[0], tcrecv.at[0], to_c)]
    beside[0].start()
    y_copies, x_copies, d_copies = [], [], []
    for p in range(mats):
        y_copies.append(remote(w_ref.at[z, p], place(x, z, y, p), ysend.at[p], yrecv.at[p], to_y))
        x_copies.append(remote(w_ref.at[z, p], place(x, z, y, p), xsend.at[p], xrecv.at[p], to_x))
        y_copies[p].start()
        x_copies[p].start()
    for d in range(1, depth):
        target = {"z": lax.rem(z + d, depth)}
        scale_sends.append(remote(s_ref, sa_ref.at[c, x, y, z], ssend.at[d], srecv.at[d], target))
        scale_sends[-1].start()
    for d in range(1, depth):
        target = lax.rem(z + d, depth)
        for p in range(mats):
            slot = d * mats + p
            z_copies.append(
                remote(w_ref.at[target, p], place(x, z, y, p), zsend.at[slot], zrecv.at[slot], {"z": target})
            )
            z_copies[-1].start()
    for d in range(1, depth):
        target = {"z": lax.rem(z + d, depth)}
        token_sends.append(remote(t_ref, ta_ref.at[d, c], tzsend.at[d], tzrecv.at[d], target))
        token_sends[-1].start()
    for d in range(1, depth):
        target = lax.rem(z + d, depth)
        m_copies.append(remote(m_ref.at[target], held_ref.at[d], msend.at[d], mrecv.at[d], {"z": target}))
        m_copies[-1].start()

    def relay(e):
        d, p = divmod(e, mats)
        source = lax.rem(z - d + depth, depth)
        if e % 2 == 0:
            y_copies[e].wait_recv()
            block = place(x, source, 1 - y, p)
            copy = remote(block, block, dsend.at[e], drecv.at[e], to_x)
        else:
            x_copies[e].wait_recv()
            block = place(1 - x, source, y, p)
            copy = remote(block, block, dsend.at[e], drecv.at[e], to_y)
        copy.start()
        d_copies.append(copy)

    keeps[0].wait()
    for copy in scale_sends:
        copy.wait()
    hops = (sa_ref.at[c, x, y], sa_ref.at[c, x], sa_ref.at[c])
    for k, (part, target) in enumerate(zip(hops, (to_y, to_x, to_c))):
        slot = (0, depth, depth + 1)[k]
        hop = remote(part, part, ssend.at[slot], srecv.at[slot], target)
        hop.start()
        hop.wait()
    count = depth * mats
    for e in range(mats, count):
        d, p = divmod(e, mats)
        block = place(x, lax.rem(z - d + depth, depth), y, p)
        z_copies[e - mats].wait_recv()
        ycopy = remote(block, block, ysend.at[e], yrecv.at[e], to_y)
        xcopy = remote(block, block, xsend.at[e], xrecv.at[e], to_x)
        ycopy.start()
        xcopy.start()
        y_copies.append(ycopy)
        x_copies.append(xcopy)
        relay(e - mats)
    for e in range(count - mats, count):
        relay(e)
    for d in range(1, depth):
        token_sends[d - 1].wait_recv()
        copy = remote(ta_ref.at[d, c], ta_ref.at[d, c], tcsend.at[d], tcrecv.at[d], to_c)
        copy.start()
        beside.append(copy)
    for e in range(count):
        (x_copies if e % 2 == 0 else y_copies)[e].wait_recv()
        d_copies[e].wait()
        y_copies[e].wait_send()
        x_copies[e].wait_send()
    for copy in beside:
        copy.wait()
    for copy in m_copies:
        copy.wait()
    for copy in z_copies + token_sends:
        copy.wait_send()
    for copy in keeps[1:]:
        copy.wait()


def spread_weights(depth, blocks, mixer_blocks, scale_block, own_rows):
    mats, rows, width = blocks.shape[1:]
    dma = pltpu.SemaphoreType.DMA
    return pl.pallas_call(
        functools.partial(weights_kernel, depth),
        out_shape=(
            jax.ShapeDtypeStruct((mats, 2, rows, depth * 2 * width), jnp.bfloat16),
            jax.ShapeDtypeStruct(mixer_blocks.shape, jnp.bfloat16),
            jax.ShapeDtypeStruct((CORES, 2, 2, depth) + scale_block.shape, jnp.float32),
            jax.ShapeDtypeStruct((depth, CORES) + own_rows.shape, jnp.bfloat16),
        ),
        in_specs=[ANY] * 4,
        out_specs=(ANY,) * 4,
        scratch_shapes=[dma((depth * mats,)) for _ in range(8)]
        + [dma((depth,)), dma((depth,))]
        + [dma((depth + 2,)), dma((depth + 2,))]
        + [dma((depth,)) for _ in range(4)]
        + [dma((4,))],
        compiler_params=pltpu.CompilerParams(collective_id=0, has_side_effects=True),
        name="spread_weights",
    )(blocks, mixer_blocks, scale_block, own_rows)


def dot_last(left, right):
    return lax.dot_general(left, right, (((1,), (1,)), ((), ())), preferred_element_type=jnp.float32)


def merged(ref, k):
    two, rows, features = ref.shape[1:]
    return ref[k].reshape(two * rows, features)


def feed_chunk(inputs, weights, factors, taps):
    gate_sum = dot_last(inputs, merged(weights, 0)) * factors[0:1]
    up_sum = dot_last(inputs, merged(weights, 1)) * factors[1:2]
    hidden = (gate_sum / (1.0 + jnp.exp(-gate_sum)) * up_sum).astype(jnp.bfloat16)
    return jnp.dot(hidden, merged(weights, 2), preferred_element_type=jnp.float32)


def mixer_chunk(inputs, weights, factors, taps):
    outgate = dot_last(inputs, merged(weights, 0)) * factors[0:1]
    ingate = dot_last(inputs, merged(weights, 1)) * factors[1:2]
    values = dot_last(inputs, merged(weights, 2)) * factors[2:3]
    mixed = ingate * values
    position = lax.rem(lax.broadcasted_iota(jnp.int32, mixed.shape, 0), LENGTH)
    convolved = taps[TAPS - 1 : TAPS] * mixed
    for back in range(1, TAPS):
        earlier = jnp.where(position >= back, pltpu.roll(mixed, back, 0), 0.0)
        convolved = convolved + taps[TAPS - 1 - back : TAPS - back] * earlier
    gated = (outgate * convolved).astype(jnp.bfloat16)
    return jnp.dot(gated, merged(weights, 3), preferred_element_type=jnp.float32)


def stage_kernel(depth, chunk, first, final, *refs):
    refs = list(refs)
    take = lambda n: [refs.pop(0) for _ in range(n)]
    w_ref, f_ref, k_ref, own_ref, scale_ref, gain_ref, shift_ref = take(7)
    if first:
        whole, held_ref = take(2)
        out_ref, m_ref = take(2)
    else:
        (out_ref,) = take(1)
    part, half, sums, got, hsend, hrecv, rsend, rrecv = take(8)
    z, c = lax.axis_index("z"), lax.axis_index("c")
    to_c = {"c": 1 - c}
    if first:
        ysend, yrecv, xsend, xrecv, dsend, drecv, local = take(7)
        y, x = lax.axis_index("y"), lax.axis_index("x")
        greet(depth, ("y", "x", "c"))
        width = held_ref.shape[-1]
        y_copies, x_copies, d_copies, keeps = [], [], [], []
        for d in range(depth):
            block = block_place(m_ref, x, lax.rem(z - d + depth, depth), y, width)
            y_copies.append(remote(held_ref.at[d], block, ysend.at[d], yrecv.at[d], {"y": 1 - y}))
            x_copies.append(remote(held_ref.at[d], block, xsend.at[d], xrecv.at[d], {"x": 1 - x}))
            keeps.append(pltpu.make_async_copy(held_ref.at[d], block, local.at[d]))
            y_copies[d].start()
            x_copies[d].start()
            keeps[d].start()
    else:
        whole, zsend, zrecv, csend, crecv = take(5)
        if final:
            sheet, fsend, frecv = take(3)
            x = lax.axis_index("x")
            greet(depth, ("x", "c"), [{"x": 1 - x, "c": 1 - c}])
        else:
            greet(depth, ("c",))
        beside = remote(own_ref, whole.at[0, c], csend.at[0], crecv.at[0], to_c)
        beside.start()
        across = []
        for d in range(1, depth):
            target = {"z": lax.rem(z + d, depth)}
            across.append(remote(own_ref, whole.at[d, c], zsend.at[d], zrecv.at[d], target))
            across[-1].start()
        whole[0, c] = own_ref[...]

    def share(d):
        target = {"z": lax.rem(z - d + depth, depth)}
        return remote(sums.at[d], got.at[d], rsend.at[d], rrecv.at[d], target)

    def handover(d):
        return remote(part.at[d, 1 - c], half.at[d], hsend.at[d], hrecv.at[d], to_c)

    def forward(d):
        return remote(whole.at[d, c], whole.at[d, c], csend.at[d], crecv.at[d], to_c)

    def step(i, carry):
        d = lax.rem(i + 1, depth) if first else i
        if not first:

            @pl.when(d > 0)
            def _():
                remote(own_ref, whole.at[d, c], zsend.at[d], zrecv.at[d], {"z": z}).wait_recv()
                forward(d).start()

            forward(d).wait_recv()
        rows = own_ref.shape[0]
        inputs = whole[d].reshape(CORES * rows, -1)
        total = chunk(inputs, w_ref, f_ref[...], k_ref[...])
        part[d] = total.astype(jnp.bfloat16).reshape(part.shape[1:])
        handover(d).start()
        handover(d).wait_recv()

        @pl.when(d > 0)
        def _():
            both = part[d, c].astype(jnp.float32) + half[d].astype(jnp.float32)
            sums[d] = both.astype(jnp.bfloat16)
            share(d).start()

        return carry

    lax.fori_loop(0, depth, step, 0)
    if first:
        for d in range(depth):
            source = lax.rem(z - d + depth, depth)
            if d % 2 == 0:
                y_copies[d].wait_recv()
                block = block_place(m_ref, x, source, 1 - y, width)
                copy = remote(block, block, dsend.at[d], drecv.at[d], {"x": 1 - x})
            else:
                x_copies[d].wait_recv()
                block = block_place(m_ref, 1 - x, source, y, width)
                copy = remote(block, block, dsend.at[d], drecv.at[d], {"y": 1 - y})
            copy.start()
            d_copies.append(copy)
    total = part[0, c].astype(jnp.float32) + half[0].astype(jnp.float32)
    for d in range(1, depth):
        share(d).wait_recv()
        total = total + got[d].astype(jnp.float32)
    summed = RESIDUAL_SCALE * own_ref[...].astype(jnp.float32) + total * scale_ref[...]
    count = summed.shape[1]
    average = jnp.sum(summed, -1, keepdims=True) / count
    mean_square = jnp.sum(summed * summed, -1, keepdims=True) / count
    variance = mean_square - average * average
    normed = (summed - average) * lax.rsqrt(variance + EPSILON) * gain_ref[...] + shift_ref[...]
    if final:
        rows, columns = own_ref.shape[0], out_ref.shape[1]
        own_place = x * CORES + c
        here = pl.ds(pl.multiple_of(own_place * rows, rows), rows)
        sheet[...] = normed.astype(jnp.bfloat16)
        leaving = []
        for k, (tx, tc) in enumerate(((1 - x, c), (1 - x, 1 - c), (x, 1 - c))):
            there = pl.ds(pl.multiple_of((tx * CORES + tc) * columns, columns), columns)
            leaving.append(
                remote(sheet.at[:, there], out_ref.at[here], fsend.at[k], frecv.at[k], {"x": tx, "c": tc})
            )
            leaving[-1].start()
        out_ref[here] = sheet[:, pl.ds(pl.multiple_of(own_place * columns, columns), columns)]
        for copy in leaving:
            copy.wait()
    else:
        out_ref[...] = normed.astype(jnp.bfloat16)
    for d in range(depth):
        handover(d).wait_send()
        if d > 0:
            share(d).wait_send()
    if first:
        for d in range(depth):
            (x_copies if d % 2 == 0 else y_copies)[d].wait_recv()
            for copy in (y_copies[d], x_copies[d]):
                copy.wait_send()
            d_copies[d].wait()
            keeps[d].wait()
    else:
        beside.wait_send()
        for d in range(1, depth):
            forward(d).wait_send()
            across[d - 1].wait_send()


def stage(depth, number, chunk, weights, factors, taps, own, scale, gain, shift, whole=None, held=None, final=False):
    rows, features = own.shape
    first = whole is not None
    dma = pltpu.SemaphoreType.DMA
    block = pltpu.VMEM((depth, rows, features), jnp.bfloat16)
    pair = pltpu.VMEM((depth, CORES, rows, features), jnp.bfloat16)
    operands = [weights, factors, taps, own, scale[None], gain[None], shift[None]]
    in_specs = [VMEM] * 7
    out_shape = [jax.ShapeDtypeStruct((rows, features), jnp.bfloat16)]
    out_specs = [VMEM]
    scratch = [pair, block, block, block] + [dma((depth,)) for _ in range(4)]
    if first:
        operands += [whole, held]
        in_specs += [VMEM, ANY]
        mats, part_rows, width = held.shape[1:]
        out_shape.append(jax.ShapeDtypeStruct((mats, 2, part_rows, depth * 2 * width), jnp.bfloat16))
        out_specs.append(ANY)
        scratch += [dma((depth,)) for _ in range(7)]
    else:
        scratch += [pair] + [dma((depth,)) for _ in range(4)]
    if final:
        out_shape = [jax.ShapeDtypeStruct((2 * CORES * rows, features // (2 * CORES)), jnp.bfloat16)]
        scratch += [pltpu.VMEM((rows, features), jnp.bfloat16), dma((3,)), dma((3,))]
    return pl.pallas_call(
        functools.partial(stage_kernel, depth, chunk, first, final),
        out_shape=tuple(out_shape),
        in_specs=in_specs,
        out_specs=tuple(out_specs),
        scratch_shapes=scratch,
        compiler_params=pltpu.CompilerParams(
            collective_id=number, has_side_effects=True, vmem_limit_bytes=40 * 1024 * 1024
        ),
        name=f"stage_{number}",
    )(*operands)


def column_plan(
    depth, tokens, gate_weight, up_weight, down_weight, gate_scale, up_scale, down_scale,
    bgate_weight, cgate_weight, value_weight, bgate_scale, cgate_scale, value_scale, conv_taps,
    mixout_weight, mixout_scale, first_gain, first_shift, mixer_gain, mixer_shift, last_gain, last_shift,
):
    z, c = lax.axis_index("z"), lax.axis_index("c")
    own = lax.all_to_all(tokens, ("x", "c"), 0, 1, tiled=True)

    def cut(matrix):
        return matrix.astype(jnp.bfloat16).reshape(depth, -1, matrix.shape[1])

    blocks = jnp.stack([cut(gate_weight.T), cut(up_weight.T), cut(down_weight)], axis=1)
    mixer_blocks = jnp.stack(
        [cut(m.T) for m in (bgate_weight, cgate_weight, value_weight)] + [cut(mixout_weight)], axis=1
    )
    channels = bgate_weight.shape[1] // depth
    pieces = (gate_scale, up_scale, down_scale, bgate_scale, cgate_scale, value_scale, mixout_scale)
    flat = jnp.concatenate([piece.reshape(-1) for piece in pieces])
    flat = jnp.pad(flat, (0, -flat.shape[0] % 1024)).reshape(-1, 128)
    feed_weights, held, scales, whole = spread_weights(depth, blocks, mixer_blocks, flat, own)
    scales = scales.reshape(scales.shape[:4] + (-1,))
    mine = lax.dynamic_index_in_dim(lax.dynamic_index_in_dim(scales, c, 0, False), z, 2, False)
    edges = [0]
    for piece in pieces:
        edges.append(edges[-1] + piece.shape[1])

    def unit_scale(k):
        return mine[:, :, edges[k] : edges[k + 1]].reshape(-1)

    def feature_scale(k):
        return scales[..., edges[k] : edges[k + 1]].transpose(1, 0, 3, 2, 4).reshape(-1)

    feed_factors = jnp.stack([unit_scale(0), unit_scale(1)])
    mixer_factors = jnp.stack([unit_scale(3), unit_scale(4), unit_scale(5)])
    down_cols, mixout_cols = HALF_STEP * feature_scale(2), feature_scale(6)
    taps = conv_taps.reshape(TAPS, 2, CORES, depth, channels)
    taps = lax.dynamic_index_in_dim(lax.dynamic_index_in_dim(taps, c, 2, False), z, 2, False)
    taps = taps.reshape(TAPS, -1)

    first, mixer_weights = stage(
        depth, 1, feed_chunk, feed_weights, feed_factors, taps, own, down_cols, first_gain, first_shift, whole, held
    )
    (second,) = stage(
        depth, 2, mixer_chunk, mixer_weights, mixer_factors, taps, first, mixout_cols, mixer_gain, mixer_shift
    )
    (last,) = stage(
        depth, 3, feed_chunk, feed_weights, feed_factors, taps, second, down_cols, last_gain, last_shift, final=True
    )
    return last


def add_rows(gathered, shard_piece):
    return jnp.dot(gathered, shard_piece, preferred_element_type=jnp.float32)


def features(inputs):
    return lax.all_gather(inputs, "tp", axis=1, tiled=True)


def post_norm(residual, branch, norm_gain, norm_shift):
    summed = RESIDUAL_SCALE * residual.astype(jnp.float32) + branch
    moments = lax.psum((jnp.sum(summed, -1), jnp.sum(summed * summed, -1)), "tp")
    feature_total = summed.shape[1] * lax.axis_size("tp")
    average = (moments[0] / feature_total)[:, None]
    mean_square = (moments[1] / feature_total)[:, None]
    variance = mean_square - average * average
    return ((summed - average) * lax.rsqrt(variance + EPSILON) * norm_gain + norm_shift).astype(
        jnp.bfloat16
    )


def spread_back(weight_cols, left_rows):
    return (
        lax.psum_scatter(
            lax.dot_general(
                weight_cols, left_rows, (((0,), (1,)), ((), ())), preferred_element_type=jnp.float32
            ).astype(jnp.bfloat16),
            "tp",
            scatter_dimension=0,
            tiled=True,
        )
        .astype(jnp.float32)
        .T
    )


def shards(
    tokens,
    gate_weight,
    up_weight,
    down_weight,
    gate_scale,
    up_scale,
    down_scale,
    bgate_weight,
    cgate_weight,
    value_weight,
    bgate_scale,
    cgate_scale,
    value_scale,
    conv_taps,
    mixout_weight,
    mixout_scale,
    first_gain,
    first_shift,
    mixer_gain,
    mixer_shift,
    last_gain,
    last_shift,
):
    scales = (
        lax.all_gather(gate_scale, "fs", axis=1, tiled=True),
        lax.all_gather(up_scale, "fs", axis=1, tiled=True),
        lax.all_gather(down_scale, "fs", axis=1, tiled=True),
        lax.all_gather(bgate_scale, "fs", axis=1, tiled=True),
        lax.all_gather(cgate_scale, "fs", axis=1, tiled=True),
        lax.all_gather(value_scale, "fs", axis=1, tiled=True),
        lax.all_gather(mixout_scale, "fs", axis=1, tiled=True),
    )
    gate_cols, up_cols, down_cols, bgate_cols, cgate_cols, value_cols, mixout_cols = [
        scale_row.reshape(-1) for scale_row in scales
    ]
    tp_index = lax.axis_index("tp")
    columns = tokens.shape[1]

    def own_part(vector):
        return lax.dynamic_slice_in_dim(vector, tp_index * columns, columns)

    gate_low = gate_weight.astype(jnp.bfloat16)
    up_low = up_weight.astype(jnp.bfloat16)
    down_low = down_weight.astype(jnp.bfloat16)
    kept_gate, kept_up = (
        lax.all_gather(gate_low, "fs", axis=0, tiled=True),
        lax.all_gather(up_low, "fs", axis=0, tiled=True),
    )
    kept_down = lax.all_gather(down_low, "fs", axis=1, tiled=True)

    def channel_mix(gathered):
        gate_sum = jnp.dot(gathered, kept_gate, preferred_element_type=jnp.float32)
        up_sum = jnp.dot(gathered, kept_up, preferred_element_type=jnp.float32)
        hidden = (jax.nn.silu(gate_sum * gate_cols) * (up_sum * up_cols)).astype(jnp.bfloat16)
        return HALF_STEP * (spread_back(kept_down, hidden) * down_cols)

    first = post_norm(
        tokens, channel_mix(features(tokens)), own_part(first_gain), own_part(first_shift)
    )
    gathered = features(first)
    bgate_low = bgate_weight.astype(jnp.bfloat16)
    channels = bgate_low.shape[1]
    outgate = add_rows(gathered, lax.all_gather(bgate_low, "fs", axis=0, tiled=True))
    ingate = add_rows(
        gathered, lax.all_gather(cgate_weight.astype(jnp.bfloat16), "fs", axis=0, tiled=True)
    )
    values = add_rows(
        gathered, lax.all_gather(value_weight.astype(jnp.bfloat16), "fs", axis=0, tiled=True)
    )
    tap_weights = lax.dynamic_slice_in_dim(conv_taps, tp_index * channels, channels, 1)
    mixed = (ingate * cgate_cols * (values * value_cols)).reshape(-1, LENGTH, channels)
    padded = jnp.pad(mixed, ((0, 0), (TAPS - 1, 0), (0, 0)))
    convolved = jnp.zeros(mixed.shape, jnp.float32)
    for tap_index in range(TAPS):
        convolved = convolved + tap_weights[tap_index] * padded[:, tap_index : tap_index + LENGTH]
    gated = (outgate * bgate_cols * convolved.reshape(-1, channels)).astype(jnp.bfloat16)
    mix_full = lax.all_gather(mixout_weight.astype(jnp.bfloat16), "fs", axis=1, tiled=True)
    second = post_norm(
        first,
        spread_back(mix_full, gated) * mixout_cols,
        own_part(mixer_gain),
        own_part(mixer_shift),
    )
    return post_norm(
        second, channel_mix(features(second)), own_part(last_gain), own_part(last_shift)
    )


def solution(mesh):
    in_specs = (
        P("fs", "tp"),
        P("fs", "tp"),
        P("fs", "tp"),
        P("tp", "fs"),
        P("tp", "fs"),
        P("tp", "fs"),
        P("tp", "fs"),
        P("fs", "tp"),
        P("fs", "tp"),
        P("fs", "tp"),
        P("tp", "fs"),
        P("tp", "fs"),
        P("tp", "fs"),
        P(),
        P("tp", "fs"),
        P("tp", "fs"),
        P(),
        P(),
        P(),
        P(),
        P(),
        P(),
    )
    out_specs = P("fs", "tp")
    across = mesh.shape["tp"] // CORES
    if across == 2 and mesh.shape["fs"] % 2 == 0 and mesh.shape["fs"] > 2:
        depth = mesh.shape["fs"] // 2
        fine = Mesh(mesh.devices.reshape(depth, 2, 2, CORES), ("z", "y", "x", "c"))
        names = {"fs": ("z", "y"), "tp": ("x", "c")}

        def split(spec):
            return P(*(names.get(name) for name in spec))

        return jax.shard_map(
            functools.partial(column_plan, depth),
            mesh=fine,
            in_specs=tuple(split(spec) for spec in in_specs),
            out_specs=split(out_specs),
            check_vma=False,
        )
    return jax.shard_map(shards, mesh=mesh, in_specs=in_specs, out_specs=out_specs, check_vma=False)
```

profile of v0, /device:TPU:1, one launch (start us, length us, event | category | flops | bytes accessed | tf_op | source)
XLA Modules:
  0.0 285.0 jit_solution(2087080414463070443)
XLA Ops:
  0.0 0.0 copy-start.13
  0.0 0.0 copy-start.14
  0.0 4.4 %all-to-all-start = ((bf16[4,64,512]{2,1,0:T(8,128)(2,1)}), bf16[4,64,512]{2,1,0:T(8,128)(2,1)S(1)}, u32[]{:S(2)}, u32[]{:S(2)}) async-start(bf16[4,64,512]{2,1,0:T(8,128)(2,1)} %bitcast.73), calls=%async_computation | async-start | bytes 524288 | tf_op jit(solution)/shard_map/all_to_all | solution.py:388
  4.4 0.8 concatenate.3
  5.2 0.6 pad_bitcast_fusion.s_ref
  5.8 0.8 reshape.63
  6.6 1.1 convert_bitcast_fusion.4
  7.7 0.0 copy-start.9
  7.7 0.8 copy.34
  8.5 0.0 copy-done.13
  8.6 0.9 copy.35
  9.4 0.0 copy-done.14
  9.5 0.8 copy.36
  10.3 1.1 convert_element_type.49
  11.4 0.0 copy-done.9
  11.4 0.1 convert_bitcast_fusion.1
  11.5 0.0 copy-start.10
  11.5 0.0 copy-start.11
  11.5 0.0 copy-start.12
  11.5 1.5 convert_bitcast_fusion
  13.0 0.0 copy-done.10
  13.0 0.0 copy-done.11
  13.0 0.0 copy-done.12
  13.1 1.1 pad_maximum_fusion.1.m_ref
  14.2 0.3 copy.32
  14.5 0.3 copy.33
  14.7 1.4 convert_element_type.42
  16.2 1.6 pad_maximum_fusion.w_ref
  17.8 0.0 all-to-all-done
  17.8 0.7 copy.45
  18.5 0.0 copy-start
  18.5 0.0 copy-start.3
  18.5 0.0 copy-start.4
  18.5 97.7 %spread_weights.1 = (bf16[3,2,352,2048]{3,2,1,0:T(8,128)(2,1)}, bf16[4,4,128,256]{3,2,1,0:T(8,128)(2,1)}, f32[2,2,2,4,8,128]{5,4,3,2,1,0:T(8,128)}, bf16[4,2,64,2048]{3,2,1,0:T(8,128)(2,1)}) custom-call(bf16[4,3,352,256]{3,2,1,0:T(8,128)(2,1)} %pad_maximum_fusion.w_ref, bf16[4,4,128,256]{3,2,1,0:T(8,128)(2,1)} %pad_maximum_fusion.1.m_ref, ...), custom_call_target="tpu_custom_call" | custom-call | tf_op jit(solution)/shard_map/spread_weights/pallas_call | solution.py:159
  116.2 0.9 reshape.62
  117.2 0.1 fusion
  117.3 0.1 fusion.1
  117.3 0.1 fusion.2
  117.4 0.1 mul.22.refs_4_
  117.5 0.1 stack_reshape.43
  117.6 0.1 stack_reshape.45
  117.7 0.1 stack_reshape.47
  117.8 0.1 stack_reshape.46
  117.9 0.1 stack_reshape.44
  117.9 0.1 broadcast_in_dim_reshape.3.refs_4_
  118.1 0.0 copy-done
  118.1 0.0 copy-done.3
  118.1 0.0 copy-done.4
  118.1 0.0 copy-start.1
  118.1 1.6 copy-done.1
  119.7 1.2 copy-done.2
  120.9 41.4 %stage_1.1 = (bf16[64,2048]{1,0:T(8,128)(2,1)S(1)}, bf16[4,2,128,2048]{3,2,1,0:T(8,128)(2,1)S(1)}) custom-call(bf16[3,2,352,2048]{3,2,1,0:T(8,128)(2,1)} %get-tuple-element.11.refs_0_, f32[2,704]{1,0:T(2,128)S(1)} %pad_maximum_fusion.2.refs_1_, f32[3,256]{1,0:T(4,128)S(1)} %bitcast.56, bf16[64,2048]{1,0:T(8,128)(2,1)S(1)} %bitcast.55, ...), custom_call_target="tpu_custom_call" | custom-call | tf_op jit(solution)/shard_map/stage_1/pallas_call | solution.py:369
  162.4 0.0 copy-done.5
  162.4 0.0 copy-done.6
  162.4 0.0 copy-start.7
  162.4 0.0 copy-start.8
  162.4 60.5 %stage_2.1.refs_3_ = bf16[64,2048]{1,0:T(8,128)(2,1)S(1)} custom-call(bf16[4,2,128,2048]{3,2,1,0:T(8,128)(2,1)S(1)} %get-tuple-element.15.refs_0_, f32[3,256]{1,0:T(4,128)S(1)} %pad_maximum_fusion.3.refs_1_, f32[3,256]{1,0:T(4,128)S(1)} %bitcast.57, bf16[64,2048]{1,0:T(8,128)(2,1)S(1)} %get-tuple-element.16.refs_3_, ...), custom_call_target="tpu_custom_call" | custom-call | tf_op jit(solution)/shard_map/stage_2/pallas_call | solution.py:369
  223.0 0.0 slice-done
  223.0 0.0 slice-done.1
  223.0 0.0 slice-done.2
  223.0 0.0 copy-done.7
  223.0 0.0 copy-done.8
  223.0 61.2 %stage_3.1 = bf16[256,512]{1,0:T(8,128)(2,1)S(1)} custom-call(bf16[3,2,352,2048]{3,2,1,0:T(8,128)(2,1)S(1)} %bitcast.53, f32[2,704]{1,0:T(2,128)S(1)} %pad_maximum_fusion.2.refs_1_, f32[3,256]{1,0:T(4,128)S(1)} %bitcast.58, bf16[64,2048]{1,0:T(8,128)(2,1)S(1)} %stage_2.1.refs_3_, f32[1,2048]{1,0:T(1,128)S(1)} %mul.22.refs_4_, f32[1,2048]{1,0:T(1,128)S(1)} %bitcast.63, ...), custom_call_target="tpu_custom_call" | custom-call | tf_op jit(solution)/shard_map/stage_3/pallas_call | solution.py:369
  284.2 0.7 copy.55
  (16 shorter events, 0.2 us)
Async XLA Ops:
  0.0 8.5 %copy-start.13 = (f32[256,512]{1,0:T(8,128)S(1)}, f32[256,512]{1,0:T(8,128)}, u32[]{:S(2)}) copy-start(f32[256,512]{1,0:T(8,128)} %param.30) | copy-start | bytes 1572868
  0.0 9.4 %copy-start.14 = (f32[256,512]{1,0:T(8,128)S(1)}, f32[256,512]{1,0:T(8,128)}, u32[]{:S(2)}) copy-start(f32[256,512]{1,0:T(8,128)} %param.31) | copy-start | bytes 1572868
  0.0 17.8 %all-to-all-start = ((bf16[4,64,512]{2,1,0:T(8,128)(2,1)}), bf16[4,64,512]{2,1,0:T(8,128)(2,1)S(1)}, u32[]{:S(2)}, u32[]{:S(2)}) async-start(bf16[4,64,512]{2,1,0:T(8,128)(2,1)} %bitcast.73), calls=%async_computation | async-start | bytes 524288 | tf_op jit(solution)/shard_map/all_to_all | solution.py:388
  7.7 3.7 %copy-start.9 = (f32[256,1408]{1,0:T(8,128)S(1)}, f32[256,1408]{1,0:T(8,128)}, u32[]{:S(2)}) copy-start(f32[256,1408]{1,0:T(8,128)} %param.23) | copy-start | bytes 4325380
  11.5 1.6 copy-start.10
  11.5 1.6 copy-start.11
  11.5 1.6 copy-start.12
  18.5 99.6 %copy-start = (bf16[4,8,8,512]{3,2,0,1:T(8,128)(2,1)S(1)}, bf16[4,8,8,512]{3,2,0,1:T(8,128)(2,1)}, u32[]{:S(2)}) copy-start(bf16[4,8,8,512]{3,2,0,1:T(8,128)(2,1)} %copy.45) | copy-start | bytes 786436
  18.5 99.6 %copy-start.3 = (f32[2048]{0:T(1024)S(1)}, f32[2048]{0:T(1024)}, u32[]{:S(2)}) copy-start(f32[2048]{0:T(1024)} %param.38) | copy-start | bytes 24580
  18.5 99.6 %copy-start.4 = (f32[2048]{0:T(1024)S(1)}, f32[2048]{0:T(1024)}, u32[]{:S(2)}) copy-start(f32[2048]{0:T(1024)} %param.39) | copy-start | bytes 24580
  117.4 105.6 %slice-start = ((s8[8650752]{0:T(1024)(128)(4,1)}), s8[262144]{0:T(1024)(128)(4,1)S(1)}, s32[]{:S(2)}) async-start(s8[8650752]{0:T(1024)(128)(4,1)} %bitcast.52), calls=%async_computation.1 | async-start | bytes 524288
  118.1 1.6 copy-start.1
  119.7 1.2 copy-start.2
  120.9 41.5 %copy-start.5 = (f32[2048]{0:T(1024)S(1)}, f32[2048]{0:T(1024)}, u32[]{:S(2)}) copy-start(f32[2048]{0:T(1024)} %param.40) | copy-start | bytes 24580
  120.9 41.5 %copy-start.6 = (f32[2048]{0:T(1024)S(1)}, f32[2048]{0:T(1024)}, u32[]{:S(2)}) copy-start(f32[2048]{0:T(1024)} %param.41) | copy-start | bytes 24580
  120.9 102.1 %slice-start.1 = ((s8[8650752]{0:T(1024)(128)(4,1)}), s8[4194304]{0:T(1024)(128)(4,1)S(1)}, s32[]{:S(2)}) async-start(s8[8650752]{0:T(1024)(128)(4,1)} %bitcast.52), calls=%async_computation.2 | async-start | bytes 8388608
  120.9 102.1 %slice-start.2 = ((s8[8650752]{0:T(1024)(128)(4,1)}), s8[4194304]{0:T(1024)(128)(4,1)S(1)}, s32[]{:S(2)}) async-start(s8[8650752]{0:T(1024)(128)(4,1)} %bitcast.52), calls=%async_computation.3 | async-start | bytes 8388608
  162.4 60.6 %copy-start.7 = (f32[2048]{0:T(1024)S(1)}, f32[2048]{0:T(1024)}, u32[]{:S(2)}) copy-start(f32[2048]{0:T(1024)} %param.42) | copy-start | bytes 24580
  162.4 60.6 %copy-start.8 = (f32[2048]{0:T(1024)S(1)}, f32[2048]{0:T(1024)}, u32[]{:S(2)}) copy-start(f32[2048]{0:T(1024)} %param.43) | copy-start | bytes 24580
where the time goes:
time: 285 us
  Pallas kernels  261 us (92%)
  local copies, waits for them, and re-layouts  11.4 us (4%)
  other arithmetic  8 us (3%)
  starting transfers between devices  4.38 us (2%)
    pallas_call x3, Pallas kernels, stage(): pl.pallas_call(functools.partial(stage_kernel, depth, chunk, first, final...  163 us
    pallas_call x1, Pallas kernels, spread_weights(): pl.pallas_call(functools.partial(weights_kernel, depth), out_shape=(jax.S...  97.7 us
  transfers between devices with their start and end apart: 1, of which 0 were waited for; matrix products, arithmetic and copies ran while one was open for 5% of the time, Pallas kernels for 0%

commit v1 on v0

--- a/solution.py
+++ b/solution.py
@@ -37,6 +37,36 @@
     )
 
 
+def line_partners(z):
+    near = z + 1 - 2 * lax.rem(z, 2)
+    return near, lax.rem(z + 2, 4), 3 - z, lax.rem((z + 1) // 2, 2)
+
+
+def line_sends(z, own, slot, send, recv):
+    near, cross, opposite, middle = line_partners(z)
+
+    @pl.when(middle == 0)
+    def _():
+        remote(own, slot(2), send.at[0], recv.at[2], {"z": cross}).start()
+
+    @pl.when(middle == 1)
+    def _():
+        remote(own, slot(3), send.at[0], recv.at[3], {"z": opposite}).start()
+
+    remote(own, slot(1), send.at[1], recv.at[1], {"z": near}).start()
+
+
+def line_waits(z, own, slot, send, recv):
+    near, cross, opposite, middle = line_partners(z)
+    for k in range(2):
+        remote(own, slot(1), send.at[k], recv.at[1], {"z": near}).wait_send()
+
+    @pl.when(middle == 1)
+    def _():
+        for e in (2, 3):
+            remote(slot(e), slot(5 - e), send.at[e + 2], recv.at[5 - e], {"z": near}).wait_send()
+
+
 def block_place(ref, px, pz, py, width):
     start = pl.multiple_of((pz * 2 + py) * width, width)
     return ref.at[:, px, :, pl.ds(start, width)]
@@ -58,7 +88,7 @@
         return g_ref.at[piece, px, :, pl.ds(start, width)]
 
     to_x, to_y, to_c = {"x": 1 - x}, {"y": 1 - y}, {"c": 1 - c}
-    scale_sends, token_sends, z_copies, m_copies = [], [], [], []
+    scale_sends, z_copies, m_copies = [], [], []
     keeps = [
         pltpu.make_async_copy(s_ref, sa_ref.at[c, x, y, z], local.at[0]),
         pltpu.make_async_copy(t_ref, ta_ref.at[0, c], local.at[1]),
@@ -87,10 +117,8 @@
                 remote(w_ref.at[target, p], place(x, z, y, p), zsend.at[slot], zrecv.at[slot], {"z": target})
             )
             z_copies[-1].start()
-    for d in range(1, depth):
-        target = {"z": lax.rem(z + d, depth)}
-        token_sends.append(remote(t_ref, ta_ref.at[d, c], tzsend.at[d], tzrecv.at[d], target))
-        token_sends[-1].start()
+    near, cross, opposite, middle = line_partners(z)
+    line_sends(z, t_ref, lambda e: ta_ref.at[e, c], tzsend, tzrecv)
     for d in range(1, depth):
         target = lax.rem(z + d, depth)
         m_copies.append(remote(m_ref.at[target], held_ref.at[d], msend.at[d], mrecv.at[d], {"z": target}))
@@ -133,9 +161,14 @@
         relay(e - mats)
     for e in range(count - mats, count):
         relay(e)
-    for d in range(1, depth):
-        token_sends[d - 1].wait_recv()
-        copy = remote(ta_ref.at[d, c], ta_ref.at[d, c], tcsend.at[d], tcrecv.at[d], to_c)
+    for e in (1, 3, 2):
+        piece = ta_ref.at[e, c]
+        remote(piece, piece, tzsend.at[e], tzrecv.at[e], {"z": near}).wait_recv()
+        if e > 1:
+            @pl.when(middle == 1)
+            def _():
+                remote(piece, ta_ref.at[5 - e, c], tzsend.at[e + 2], tzrecv.at[5 - e], {"z": near}).start()
+        copy = remote(piece, piece, tcsend.at[e], tcrecv.at[e], to_c)
         copy.start()
         beside.append(copy)
     for e in range(count):
@@ -147,8 +180,9 @@
         copy.wait()
     for copy in m_copies:
         copy.wait()
-    for copy in z_copies + token_sends:
+    for copy in z_copies:
         copy.wait_send()
+    line_waits(z, t_ref, lambda e: ta_ref.at[e, c], tzsend, tzrecv)
     for copy in keeps[1:]:
         copy.wait()
 
@@ -169,7 +203,7 @@
         scratch_shapes=[dma((depth * mats,)) for _ in range(8)]
         + [dma((depth,)), dma((depth,))]
         + [dma((depth + 2,)), dma((depth + 2,))]
-        + [dma((depth,)) for _ in range(4)]
+        + [dma((depth + 2,)) for _ in range(4)]
         + [dma((4,))],
         compiler_params=pltpu.CompilerParams(collective_id=0, has_side_effects=True),
         name="spread_weights",
@@ -215,8 +249,9 @@
         out_ref, m_ref = take(2)
     else:
         (out_ref,) = take(1)
-    part, half, sums, got, hsend, hrecv, rsend, rrecv = take(8)
+    part, half, sums, got, extra, hsend, hrecv, rsend, rrecv, esend, erecv = take(11)
     z, c = lax.axis_index("z"), lax.axis_index("c")
+    near, cross, opposite, middle = line_partners(z)
     to_c = {"c": 1 - c}
     if first:
         ysend, yrecv, xsend, xrecv, dsend, drecv, local = take(7)
@@ -242,16 +277,20 @@
             greet(depth, ("c",))
         beside = remote(own_ref, whole.at[0, c], csend.at[0], crecv.at[0], to_c)
         beside.start()
-        across = []
-        for d in range(1, depth):
-            target = {"z": lax.rem(z + d, depth)}
-            across.append(remote(own_ref, whole.at[d, c], zsend.at[d], zrecv.at[d], target))
-            across[-1].start()
+        line_sends(z, own_ref, lambda e: whole.at[e, c], zsend, zrecv)
         whole[0, c] = own_ref[...]
 
-    def share(d):
-        target = {"z": lax.rem(z - d + depth, depth)}
-        return remote(sums.at[d], got.at[d], rsend.at[d], rrecv.at[d], target)
+    def to_near(d):
+        return remote(sums.at[d], got.at[1], rsend.at[d], rrecv.at[1], {"z": near})
+
+    def to_merge(d):
+        return remote(sums.at[d], extra.at[5 - d], rsend.at[d], erecv.at[5 - d], {"z": near})
+
+    def to_cross():
+        return remote(sums.at[2], got.at[2], rsend.at[2], rrecv.at[2], {"z": cross})
+
+    def to_opposite():
+        return remote(sums.at[3], got.at[3], rsend.at[3], rrecv.at[3], {"z": opposite})
 
     def handover(d):
         return remote(part.at[d, 1 - c], half.at[d], hsend.at[d], hrecv.at[d], to_c)
@@ -260,12 +299,19 @@
         return remote(whole.at[d, c], whole.at[d, c], csend.at[d], crecv.at[d], to_c)
 
     def step(i, carry):
-        d = lax.rem(i + 1, depth) if first else i
-        if not first:
+        if first:
+            d = (1 - middle) * (3 - i) + middle * lax.rem(i + 1, depth)
+        else:
+            d = i + middle * (i // 2) * (5 - 2 * i)
 
             @pl.when(d > 0)
             def _():
-                remote(own_ref, whole.at[d, c], zsend.at[d], zrecv.at[d], {"z": z}).wait_recv()
+                remote(own_ref, whole.at[d, c], zsend.at[0], zrecv.at[d], {"z": near}).wait_recv()
+
+                @pl.when(middle * d > 1)
+                def _():
+                    remote(whole.at[d, c], whole.at[5 - d, c], zsend.at[d + 2], zrecv.at[5 - d], {"z": near}).start()
+
                 forward(d).start()
 
             forward(d).wait_recv()
@@ -280,7 +326,14 @@
         def _():
             both = part[d, c].astype(jnp.float32) + half[d].astype(jnp.float32)
             sums[d] = both.astype(jnp.bfloat16)
-            share(d).start()
+
+        @pl.when(d == 1)
+        def _():
+            to_near(1).start()
+
+        @pl.when((1 - middle) * d > 1)
+        def _():
+            to_merge(d).start()
 
         return carry
 
@@ -298,10 +351,21 @@
                 copy = remote(block, block, dsend.at[d], drecv.at[d], {"y": 1 - y})
             copy.start()
             d_copies.append(copy)
+
+    @pl.when(middle == 1)
+    def _():
+        for d, leave in ((2, to_cross), (3, to_opposite)) if first else ((3, to_opposite), (2, to_cross)):
+            remote(sums.at[d], extra.at[d], esend.at[d], erecv.at[d], {"z": near}).wait_recv()
+            both = part[d, c].astype(jnp.float32) + half[d].astype(jnp.float32) + extra[d].astype(jnp.float32)
+            sums[d] = both.astype(jnp.bfloat16)
+            leave().start()
+
     total = part[0, c].astype(jnp.float32) + half[0].astype(jnp.float32)
-    for d in range(1, depth):
-        share(d).wait_recv()
-        total = total + got[d].astype(jnp.float32)
+    to_near(1).wait_recv()
+    total = total + got[1].astype(jnp.float32)
+    last = 2 + middle
+    remote(sums.at[last], got.at[last], rsend.at[last], rrecv.at[last], {"z": near}).wait_recv()
+    total = total + got[last].astype(jnp.float32)
     summed = RESIDUAL_SCALE * own_ref[...].astype(jnp.float32) + total * scale_ref[...]
     count = summed.shape[1]
     average = jnp.sum(summed, -1, keepdims=True) / count
@@ -328,7 +392,7 @@
     for d in range(depth):
         handover(d).wait_send()
         if d > 0:
-            share(d).wait_send()
+            to_near(d).wait_send()
     if first:
         for d in range(depth):
             (x_copies if d % 2 == 0 else y_copies)[d].wait_recv()
@@ -340,7 +404,7 @@
         beside.wait_send()
         for d in range(1, depth):
             forward(d).wait_send()
-            across[d - 1].wait_send()
+        line_waits(z, own_ref, lambda e: whole.at[e, c], zsend, zrecv)
 
 
 def stage(depth, number, chunk, weights, factors, taps, own, scale, gain, shift, whole=None, held=None, final=False):
@@ -353,7 +417,7 @@
     in_specs = [VMEM] * 7
     out_shape = [jax.ShapeDtypeStruct((rows, features), jnp.bfloat16)]
     out_specs = [VMEM]
-    scratch = [pair, block, block, block] + [dma((depth,)) for _ in range(4)]
+    scratch = [pair, block, block, block, block] + [dma((depth,)) for _ in range(6)]
     if first:
         operands += [whole, held]
         in_specs += [VMEM, ANY]
@@ -362,7 +426,7 @@
         out_specs.append(ANY)
         scratch += [dma((depth,)) for _ in range(7)]
     else:
-        scratch += [pair] + [dma((depth,)) for _ in range(4)]
+        scratch += [pair] + [dma((depth + 2,)) for _ in range(4)]
     if final:
         out_shape = [jax.ShapeDtypeStruct((2 * CORES * rows, features // (2 * CORES)), jnp.bfloat16)]
         scratch += [pltpu.VMEM((rows, features), jnp.bfloat16), dma((3,)), dma((3,))]
@@ -581,7 +645,7 @@
     )
     out_specs = P("fs", "tp")
     across = mesh.shape["tp"] // CORES
-    if across == 2 and mesh.shape["fs"] % 2 == 0 and mesh.shape["fs"] > 2:
+    if across == 2 and mesh.shape["fs"] == 8:
         depth = mesh.shape["fs"] // 2
         fine = Mesh(mesh.devices.reshape(depth, 2, 2, CORES), ("z", "y", "x", "c"))
         names = {"fs": ("z", "y"), "tp": ("x", "c")}

time: 285 us -> 292 us (1.025)
  Pallas kernels: 261 us -> 268 us
    pallas_call x1, Pallas kernels: 97.7 us -> 105 us  [spread_weights(): pl.pallas_call(functools.partial(weights_kernel, depth), out_shape=(jax.S...]
where the time goes in v1:
time: 292 us
  Pallas kernels  268 us (92%)
  local copies, waits for them, and re-layouts  11.4 us (4%)
  other arithmetic  8 us (3%)
  starting transfers between devices  4.38 us (2%)
    pallas_call x3, Pallas kernels, stage(): pl.pallas_call(functools.partial(stage_kernel, depth, chunk, first, final...  162 us
    pallas_call x1, Pallas kernels, spread_weights(): pl.pallas_call(functools.partial(weights_kernel, depth), out_shape=(jax.S...  105 us
  transfers between devices with their start and end apart: 1, of which 0 were waited for; matrix products, arithmetic and copies ran while one was open for 5% of the time, Pallas kernels for 0%

profile of v1, /device:TPU:1, one launch (start us, length us, event | category | flops | bytes accessed | tf_op | source)
XLA Modules:
  0.0 291.7 jit_solution(3010089510186951559)
XLA Ops:
  0.0 0.0 copy-start.13
  0.0 0.0 copy-start.14
  0.0 4.4 %all-to-all-start = ((bf16[4,64,512]{2,1,0:T(8,128)(2,1)}), bf16[4,64,512]{2,1,0:T(8,128)(2,1)S(1)}, u32[]{:S(2)}, u32[]{:S(2)}) async-start(bf16[4,64,512]{2,1,0:T(8,128)(2,1)} %bitcast.73), calls=%async_computation | async-start | bytes 524288 | tf_op jit(solution)/shard_map/all_to_all | solution.py:452
  4.4 0.8 concatenate.3
  5.2 0.6 pad_bitcast_fusion.s_ref
  5.8 0.8 reshape.63
  6.6 1.1 convert_bitcast_fusion.4
  7.7 0.0 copy-start.9
  7.7 0.8 copy.34
  8.5 0.0 copy-done.13
  8.6 0.9 copy.35
  9.4 0.0 copy-done.14
  9.5 0.8 copy.36
  10.3 1.1 convert_element_type.49
  11.4 0.0 copy-done.9
  11.4 0.1 convert_bitcast_fusion.1
  11.5 0.0 copy-start.10
  11.5 0.0 copy-start.11
  11.5 0.0 copy-start.12
  11.5 1.5 convert_bitcast_fusion
  13.0 0.0 copy-done.10
  13.0 0.0 copy-done.11
  13.0 0.0 copy-done.12
  13.1 1.1 pad_maximum_fusion.1.m_ref
  14.2 0.3 copy.32
  14.5 0.3 copy.33
  14.7 1.4 convert_element_type.42
  16.2 1.6 pad_maximum_fusion.w_ref
  17.8 0.0 all-to-all-done
  17.8 0.7 copy.45
  18.5 0.0 copy-start
  18.5 0.0 copy-start.3
  18.5 0.0 copy-start.4
  18.5 105.4 %spread_weights.1 = (bf16[3,2,352,2048]{3,2,1,0:T(8,128)(2,1)}, bf16[4,4,128,256]{3,2,1,0:T(8,128)(2,1)}, f32[2,2,2,4,8,128]{5,4,3,2,1,0:T(8,128)}, bf16[4,2,64,2048]{3,2,1,0:T(8,128)(2,1)}) custom-call(bf16[4,3,352,256]{3,2,1,0:T(8,128)(2,1)} %pad_maximum_fusion.w_ref, bf16[4,4,128,256]{3,2,1,0:T(8,128)(2,1)} %pad_maximum_fusion.1.m_ref, ...), custom_call_target="tpu_custom_call" | custom-call | tf_op jit(solution)/shard_map/spread_weights/pallas_call | solution.py:193
  123.9 0.9 reshape.62
  124.9 0.1 fusion
  125.0 0.1 fusion.1
  125.1 0.1 fusion.2
  125.2 0.1 mul.22.refs_4_
  125.2 0.1 stack_reshape.43
  125.3 0.1 stack_reshape.45
  125.4 0.1 stack_reshape.47
  125.5 0.1 stack_reshape.46
  125.6 0.1 stack_reshape.44
  125.7 0.1 broadcast_in_dim_reshape.3.refs_4_
  125.8 0.0 copy-done
  125.8 0.0 copy-done.3
  125.8 0.0 copy-done.4
  125.8 0.0 copy-start.1
  125.8 1.6 copy-done.1
  127.4 1.2 copy-done.2
  128.6 41.0 %stage_1.1 = (bf16[64,2048]{1,0:T(8,128)(2,1)S(1)}, bf16[4,2,128,2048]{3,2,1,0:T(8,128)(2,1)S(1)}) custom-call(bf16[3,2,352,2048]{3,2,1,0:T(8,128)(2,1)} %get-tuple-element.11.refs_0_, f32[2,704]{1,0:T(2,128)S(1)} %pad_maximum_fusion.2.refs_1_, f32[3,256]{1,0:T(4,128)S(1)} %bitcast.56, bf16[64,2048]{1,0:T(8,128)(2,1)S(1)} %bitcast.55, ...), custom_call_target="tpu_custom_call" | custom-call | tf_op jit(solution)/shard_map/stage_1/pallas_call | solution.py:433
  169.7 0.0 copy-done.5
  169.7 0.0 copy-done.6
  169.7 0.0 copy-start.7
  169.7 0.0 copy-start.8
  169.7 56.4 %stage_2.1.refs_3_ = bf16[64,2048]{1,0:T(8,128)(2,1)S(1)} custom-call(bf16[4,2,128,2048]{3,2,1,0:T(8,128)(2,1)S(1)} %get-tuple-element.15.refs_0_, f32[3,256]{1,0:T(4,128)S(1)} %pad_maximum_fusion.3.refs_1_, f32[3,256]{1,0:T(4,128)S(1)} %bitcast.57, bf16[64,2048]{1,0:T(8,128)(2,1)S(1)} %get-tuple-element.16.refs_3_, ...), custom_call_target="tpu_custom_call" | custom-call | tf_op jit(solution)/shard_map/stage_2/pallas_call | solution.py:433
  226.2 0.0 slice-done
  226.2 0.0 slice-done.1
  226.2 0.0 slice-done.2
  226.2 0.0 copy-done.7
  226.2 0.0 copy-done.8
  226.2 64.7 %stage_3.1 = bf16[256,512]{1,0:T(8,128)(2,1)S(1)} custom-call(bf16[3,2,352,2048]{3,2,1,0:T(8,128)(2,1)S(1)} %bitcast.53, f32[2,704]{1,0:T(2,128)S(1)} %pad_maximum_fusion.2.refs_1_, f32[3,256]{1,0:T(4,128)S(1)} %bitcast.58, bf16[64,2048]{1,0:T(8,128)(2,1)S(1)} %stage_2.1.refs_3_, f32[1,2048]{1,0:T(1,128)S(1)} %mul.22.refs_4_, f32[1,2048]{1,0:T(1,128)S(1)} %bitcast.63, ...), custom_call_target="tpu_custom_call" | custom-call | tf_op jit(solution)/shard_map/stage_3/pallas_call | solution.py:433
  291.0 0.7 copy.55
  (16 shorter events, 0.2 us)
Async XLA Ops:
  0.0 8.5 %copy-start.13 = (f32[256,512]{1,0:T(8,128)S(1)}, f32[256,512]{1,0:T(8,128)}, u32[]{:S(2)}) copy-start(f32[256,512]{1,0:T(8,128)} %param.30) | copy-start | bytes 1572868
  0.0 9.4 %copy-start.14 = (f32[256,512]{1,0:T(8,128)S(1)}, f32[256,512]{1,0:T(8,128)}, u32[]{:S(2)}) copy-start(f32[256,512]{1,0:T(8,128)} %param.31) | copy-start | bytes 1572868
  0.0 17.8 %all-to-all-start = ((bf16[4,64,512]{2,1,0:T(8,128)(2,1)}), bf16[4,64,512]{2,1,0:T(8,128)(2,1)S(1)}, u32[]{:S(2)}, u32[]{:S(2)}) async-start(bf16[4,64,512]{2,1,0:T(8,128)(2,1)} %bitcast.73), calls=%async_computation | async-start | bytes 524288 | tf_op jit(solution)/shard_map/all_to_all | solution.py:452
  7.7 3.7 %copy-start.9 = (f32[256,1408]{1,0:T(8,128)S(1)}, f32[256,1408]{1,0:T(8,128)}, u32[]{:S(2)}) copy-start(f32[256,1408]{1,0:T(8,128)} %param.23) | copy-start | bytes 4325380
  11.5 1.6 copy-start.10
  11.5 1.6 copy-start.11
  11.5 1.6 copy-start.12
  18.5 107.3 %copy-start = (bf16[4,8,8,512]{3,2,0,1:T(8,128)(2,1)S(1)}, bf16[4,8,8,512]{3,2,0,1:T(8,128)(2,1)}, u32[]{:S(2)}) copy-start(bf16[4,8,8,512]{3,2,0,1:T(8,128)(2,1)} %copy.45) | copy-start | bytes 786436
  18.5 107.3 %copy-start.3 = (f32[2048]{0:T(1024)S(1)}, f32[2048]{0:T(1024)}, u32[]{:S(2)}) copy-start(f32[2048]{0:T(1024)} %param.38) | copy-start | bytes 24580
  18.5 107.3 %copy-start.4 = (f32[2048]{0:T(1024)S(1)}, f32[2048]{0:T(1024)}, u32[]{:S(2)}) copy-start(f32[2048]{0:T(1024)} %param.39) | copy-start | bytes 24580
  125.1 101.1 %slice-start = ((s8[8650752]{0:T(1024)(128)(4,1)}), s8[262144]{0:T(1024)(128)(4,1)S(1)}, s32[]{:S(2)}) async-start(s8[8650752]{0:T(1024)(128)(4,1)} %bitcast.52), calls=%async_computation.1 | async-start | bytes 524288
  125.8 1.6 copy-start.1
  127.4 1.2 copy-start.2
  128.6 41.0 %copy-start.5 = (f32[2048]{0:T(1024)S(1)}, f32[2048]{0:T(1024)}, u32[]{:S(2)}) copy-start(f32[2048]{0:T(1024)} %param.40) | copy-start | bytes 24580
  128.6 41.1 %copy-start.6 = (f32[2048]{0:T(1024)S(1)}, f32[2048]{0:T(1024)}, u32[]{:S(2)}) copy-start(f32[2048]{0:T(1024)} %param.41) | copy-start | bytes 24580
  128.6 97.6 %slice-start.1 = ((s8[8650752]{0:T(1024)(128)(4,1)}), s8[4194304]{0:T(1024)(128)(4,1)S(1)}, s32[]{:S(2)}) async-start(s8[8650752]{0:T(1024)(128)(4,1)} %bitcast.52), calls=%async_computation.2 | async-start | bytes 8388608
  128.6 97.6 %slice-start.2 = ((s8[8650752]{0:T(1024)(128)(4,1)}), s8[4194304]{0:T(1024)(128)(4,1)S(1)}, s32[]{:S(2)}) async-start(s8[8650752]{0:T(1024)(128)(4,1)} %bitcast.52), calls=%async_computation.3 | async-start | bytes 8388608
  169.7 56.5 %copy-start.7 = (f32[2048]{0:T(1024)S(1)}, f32[2048]{0:T(1024)}, u32[]{:S(2)}) copy-start(f32[2048]{0:T(1024)} %param.42) | copy-start | bytes 24580
  169.7 56.5 %copy-start.8 = (f32[2048]{0:T(1024)S(1)}, f32[2048]{0:T(1024)}, u32[]{:S(2)}) copy-start(f32[2048]{0:T(1024)} %param.43) | copy-start | bytes 24580

commit v2 on v0

v2 whole, which is shorter than its diff:
```python
import functools

import jax
import jax.numpy as jnp
from jax import lax
from jax.experimental import pallas as pl
from jax.experimental.pallas import tpu as pltpu
from jax.sharding import Mesh
from jax.sharding import PartitionSpec as P

TAPS = 3
LENGTH = 128
CORES = 2

RESIDUAL_SCALE = 1.4142135623730951
HALF_STEP = 0.5
EPSILON = 1e-05
BY_AXIS = pl.DeviceIdType.MESH
ANY = pl.BlockSpec(memory_space=pl.ANY)
VMEM = pl.BlockSpec(memory_space=pltpu.VMEM)


def remote(src, dst, send, recv, target):
    return pltpu.make_async_remote_copy(
        src_ref=src, dst_ref=dst, send_sem=send, recv_sem=recv, device_id=target, device_id_type=BY_AXIS
    )


def dot_last(left, right):
    return lax.dot_general(left, right, (((1,), (1,)), ((), ())), preferred_element_type=jnp.float32)


def merged(ref, k):
    two, rows, features = ref.shape[1:]
    return ref[k].reshape(two * rows, features)


def feed_units(inputs, weights, factors, taps):
    gate_sum = dot_last(inputs, merged(weights, 0)) * factors[0:1]
    up_sum = dot_last(inputs, merged(weights, 1)) * factors[1:2]
    return (gate_sum / (1.0 + jnp.exp(-gate_sum)) * up_sum).astype(jnp.bfloat16)


def mixer_units(inputs, weights, factors, taps):
    outgate = dot_last(inputs, merged(weights, 0)) * factors[2:3]
    ingate = dot_last(inputs, merged(weights, 1)) * factors[3:4]
    values = dot_last(inputs, merged(weights, 2)) * factors[4:5]
    mixed = ingate * values
    position = lax.rem(lax.broadcasted_iota(jnp.int32, mixed.shape, 0), LENGTH)
    convolved = taps[TAPS - 1 : TAPS] * mixed
    for back in range(1, TAPS):
        earlier = jnp.where(position >= back, pltpu.roll(mixed, back, 0), 0.0)
        convolved = convolved + taps[TAPS - 1 - back : TAPS - back] * earlier
    return (outgate * convolved).astype(jnp.bfloat16)


def later_third(i):
    return i + (i // 2) * (5 - 2 * i)


def layer_kernel(
    tokens_ref, gate_ref, up_ref, down_ref, b_ref, c_ref, v_ref, mix_ref, *refs
):
    refs = list(refs)
    take = lambda n: [refs.pop(0) for _ in range(n)]
    scale_refs = take(7)
    taps_ref = take(1)[0]
    norms = [take(2) for _ in range(3)]
    (out_ref,) = take(1)
    tin, gate_full, up_full, down_full, *mixer_full = take(8)
    wsend, msend, feed_w, mixer_w, pack, blocks, lanes, units, channels, taps_own = take(10)
    own0, own1, own2, sheet = take(4)
    stages = [dict(zip(("whole", "part", "half", "sums", "extra", "got"), take(6))) for _ in range(3)]
    local, asend, arecv, ssend, srecv, fsend, frecv = take(7)
    zsend, zrecv, ysend, yrecv, xsend, xrecv, dsend, drecv = take(8)
    mzsend, mzrecv, mysend, myrecv, mxsend, mxrecv, mdsend, mdrecv = take(8)
    for state in stages:
        names = ("rs", "rr", "ls", "lr", "cs", "cr", "hs", "hr", "ps", "gr", "er")
        state.update(zip(names, take(len(names))))

    z, y, x, c = (lax.axis_index(axis) for axis in ("z", "y", "x", "c"))
    near = z + 1 - 2 * lax.rem(z, 2)
    cross = lax.rem(z + 2, 4)
    opposite = 3 - z
    middle = lax.rem((z + 1) // 2, 2)
    partner = (z, near, cross, opposite)
    to_x, to_y, to_c = {"x": 1 - x}, {"y": 1 - y}, {"c": 1 - c}

    def partner_of(e):
        odd = 1 - 2 * lax.rem(z, 2)
        return lax.rem(z + odd * lax.rem(e, 2) + 2 * (e // 2), 4)

    loads = [
        pltpu.make_async_copy(src, dst, local.at[k])
        for k, (src, dst) in enumerate(
            zip(
                (tokens_ref, down_ref, gate_ref, up_ref, b_ref, c_ref, v_ref, mix_ref),
                (tin, down_full, gate_full, up_full, *mixer_full),
            )
        )
    ]
    for load in loads:
        load.start()
    barrier = pltpu.get_barrier_semaphore()
    greeted = [{"z": t} for t in partner[1:]] + [to_x, to_y, to_c, {"x": 1 - x, "c": 1 - c}]
    for target in greeted:
        pl.semaphore_signal(barrier, inc=1, device_id=target, device_id_type=BY_AXIS)
    pack[...] = jnp.zeros_like(pack)
    for k, scale_ref in enumerate(scale_refs):
        pack[k : k + 1, 0 : scale_ref.shape[1]] = scale_ref[...]
    pl.semaphore_wait(barrier, len(greeted))

    rows, features = own0.shape
    columns = tin.shape[1]
    place_here = x * CORES + c

    def strip(t, width):
        return pl.ds(pl.multiple_of(t * width, width), width)

    loads[0].wait()
    trades = []
    for k, (tx, tc) in enumerate(((1 - x, c), (1 - x, 1 - c), (x, 1 - c))):
        trades.append(
            remote(
                tin.at[strip(tx * CORES + tc, rows)],
                own0.at[:, strip(place_here, columns)],
                asend.at[k],
                arecv.at[k],
                {"x": tx, "c": tc},
            )
        )
        trades[-1].start()
    own0[:, strip(place_here, columns)] = tin[strip(place_here, rows)]

    hidden_rows, width = feed_w.shape[2], wsend.shape[2]
    channel_rows = mixer_w.shape[2]

    def place(p, px, pz, py):
        return feed_w.at[p, px, :, strip(pz * 2 + py, width)]

    def y_copy(e, p, src=None):
        dst = place(p, x, partner[e], y)
        return remote(dst if src is None else src, dst, ysend.at[e * 3 + p], yrecv.at[e * 3 + p], to_y)

    def x_copy(e, p, src=None):
        dst = place(p, x, partner[e], y)
        return remote(dst if src is None else src, dst, xsend.at[e * 3 + p], xrecv.at[e * 3 + p], to_x)

    def z_copy(e, p):
        src = wsend.at[p, strip(partner[e], hidden_rows)]
        return remote(src, place(p, x, z, y), zsend.at[e * 3 + p], zrecv.at[e * 3 + p], {"z": partner[e]})

    def z_landed(e, p):
        dst = place(p, x, partner[e], y)
        return remote(dst, dst, zsend.at[e * 3 + p], zrecv.at[e * 3 + p], {"z": partner[e]})

    def d_copy(e, p):
        k = e * 3 + p
        if (e + p) % 2 == 0:
            block = place(p, x, partner[e], 1 - y)
            return remote(block, block, dsend.at[k], drecv.at[k], to_x)
        block = place(p, 1 - x, partner[e], y)
        return remote(block, block, dsend.at[k], drecv.at[k], to_y)

    def relay(e, p):
        (y_copy if (e + p) % 2 == 0 else x_copy)(e, p).wait_recv()
        d_copy(e, p).start()

    def turned(src, dst, p):
        def turn(j, carry):
            here = strip(j, 128)
            dst[p, here, :] = src[:, here].T.astype(jnp.bfloat16)
            return carry

        lax.fori_loop(0, src.shape[1] // 128, turn, 0)

    order = (2, 0, 1)
    for p, full in zip(order, (down_full, gate_full, up_full)):
        loads[(2, 3, 1)[p]].wait()
        if p == 2:
            wsend[p] = full[...].astype(jnp.bfloat16)
        else:
            turned(full, wsend, p)
        mine = wsend.at[p, strip(z, hidden_rows)]
        y_copy(0, p, mine).start()
        x_copy(0, p, mine).start()
        for e in (1, 3, 2):
            z_copy(e, p).start()
    for p in order:
        feed_w[p, x, :, strip(z * 2 + y, width)] = wsend[p, strip(z, hidden_rows)]

    scale_sends = []
    for e in (1, 2, 3):
        scale_sends.append(remote(pack, blocks.at[c, x, y, z], ssend.at[e], srecv.at[e], {"z": partner[e]}))
        scale_sends[-1].start()
    blocks[c, x, y, z] = pack[...]

    def piece(state, s, h):
        return state["whole"].at[s, c, pl.ds(h * (rows // 2), rows // 2)]

    def spread(state, own):
        state["own"] = own
        for h in range(2):
            src = own.at[pl.ds(h * (rows // 2), rows // 2)]

            @pl.when(z < 3)
            def _():
                remote(src, piece(state, z, h), state["rs"].at[h], state["rr"].at[2 + h], {"z": z + 1}).start()

            @pl.when(z > 0)
            def _():
                remote(src, piece(state, z, h), state["ls"].at[h], state["lr"].at[2 + h], {"z": z - 1}).start()

        for h in range(2):
            src = own.at[pl.ds(h * (rows // 2), rows // 2)]
            remote(src, piece(state, z, h), state["cs"].at[z * 2 + h], state["cr"].at[z * 2 + h], to_c).start()
        state["whole"][z, c] = own[...]

    def beside(state, s, h):
        src = piece(state, s, h)
        return remote(src, src, state["cs"].at[s * 2 + h], state["cr"].at[s * 2 + h], to_c)

    def pass_on(state, k, h):
        slot = k * 2 + h

        @pl.when(z >= k)
        def _():
            s = lax.rem(z - k + 4, 4)
            src = piece(state, s, h)
            remote(src, src, state["rs"].at[slot], state["rr"].at[slot], to_c).wait_recv()

            @pl.when(z < 3)
            def _():
                remote(src, src, state["rs"].at[slot], state["rr"].at[slot + 2], {"z": z + 1}).start()

            beside(state, s, h).start()

        @pl.when(z + k < 4)
        def _():
            s = lax.rem(z + k, 4)
            src = piece(state, s, h)
            remote(src, src, state["ls"].at[slot], state["lr"].at[slot], to_c).wait_recv()

            @pl.when(z > 0)
            def _():
                remote(src, src, state["ls"].at[slot], state["lr"].at[slot + 2], {"z": z - 1}).start()

            beside(state, s, h).start()

    def spread_done(state):
        for k in range(4):
            for h in range(2):
                slot = k * 2 + h
                src = piece(state, z, h)

                @pl.when((z >= k) & (z < 3))
                def _():
                    remote(src, src, state["rs"].at[slot], state["rr"].at[slot], to_c).wait_send()

                @pl.when((z + k < 4) & (z > 0))
                def _():
                    remote(src, src, state["ls"].at[slot], state["lr"].at[slot], to_c).wait_send()

                beside(state, k, h).wait_send()

    for k, full in enumerate(mixer_full):
        loads[4 + k].wait()
        if k == 3:
            msend[k] = full[...].astype(jnp.bfloat16)
        else:
            turned(full, msend, k)
    for copy in trades:
        copy.wait_recv()
    spread(stages[0], own0)

    def m_place(px, pz, py):
        return mixer_w.at[:, px, :, strip(pz * 2 + py, width)]

    def m_y(e, src=None):
        dst = m_place(x, partner_of(e), y)
        return remote(dst if src is None else src, dst, mysend.at[e], myrecv.at[e], to_y)

    def m_x(e, src=None):
        dst = m_place(x, partner_of(e), y)
        return remote(dst if src is None else src, dst, mxsend.at[e], mxrecv.at[e], to_x)

    def m_z(e):
        src = msend.at[:, strip(partner_of(e), channel_rows)]
        return remote(src, m_place(x, z, y), mzsend.at[e], mzrecv.at[e], {"z": partner_of(e)})

    def m_d(e):
        if e % 2 == 0:
            block = m_place(x, partner[e], 1 - y)
            return remote(block, block, mdsend.at[e], mdrecv.at[e], to_x)
        block = m_place(1 - x, partner[e], y)
        return remote(block, block, mdsend.at[e], mdrecv.at[e], to_y)

    def m_relay(e):
        (m_y if e % 2 == 0 else m_x)(e).wait_recv()
        m_d(e).start()

    hops = [
        remote(part, part, ssend.at[slot], srecv.at[slot], target)
        for slot, (part, target) in zip(
            (0, 4, 5), ((blocks.at[c, x, y], to_y), (blocks.at[c, x], to_x), (blocks.at[c], to_c))
        )
    ]
    sent = [(0, p) for p in order]
    arriving = [(e, p) for p in order for e in (1, 3, 2)]
    for j, (e, p) in enumerate(arriving):
        z_landed(e, p).wait_recv()
        y_copy(e, p).start()
        x_copy(e, p).start()
        sent.append((e, p))
        relay(*sent[j])
        if j == 2:
            for copy in scale_sends:
                copy.wait_recv()
            hops[0].start()
        if j in (4, 6):
            hops[j // 2 - 2].wait_recv()
            hops[j // 2 - 1].start()
    for k in range(1, 4):
        for h in range(2):
            pass_on(stages[0], k, h)
    for e in (1, 3, 2):
        m_z(e).start()
    mine = msend.at[:, strip(z, channel_rows)]
    mixer_w[:, x, :, strip(z * 2 + y, width)] = msend[:, strip(z, channel_rows)]
    hops[2].wait_recv()

    wide = units.shape[1]
    unit_total = jnp.zeros(units.shape, jnp.float32)
    channel_total = jnp.zeros(channels.shape, jnp.float32)
    unit_part = scale_refs[0].shape[1]
    lane_part = scale_refs[2].shape[1]
    for px in range(2):
        for py in range(2):
            block = blocks[c, px, py, z]
            padded = jnp.concatenate([block, jnp.zeros((block.shape[0], wide - block.shape[1]), jnp.float32)], 1)
            k = px * 2 + py
            unit_total = unit_total + (pltpu.roll(padded, k * unit_part, 1) if k else padded)
            channel_total = channel_total + (pltpu.roll(block, k * lane_part, 1) if k else block)
    units[...] = unit_total
    channels[...] = channel_total
    pair = 2 * lane_part
    for px in range(2):
        for pc in range(CORES):
            for pz in range(4):
                low, high = (blocks[pc, px, py, pz][:, 0:pair] for py in range(2))
                start = ((px * CORES + pc) * 4 + pz) * pair
                lanes[:, start : start + pair] = low + pltpu.roll(high, lane_part, 1)
    for px in range(2):
        taps_own[:, px * pair : (px + 1) * pair] = taps_ref[:, strip((px * CORES + c) * 4 + z, pair)]

    for e, p in sent[len(arriving) :]:
        relay(e, p)
    m_y(0, mine).start()
    m_x(0, mine).start()
    for e, p in sent:
        (x_copy if (e + p) % 2 == 0 else y_copy)(e, p).wait_recv()
        d_copy(e, p).wait_recv()

    half_width = features // 2

    def to_near(state, e, h):
        return remote(
            state["sums"].at[e, h], state["got"].at[0, h], state["ps"].at[e * 2 + h], state["gr"].at[h], {"z": near}
        )

    def to_merge(state, e, h):
        slot = (5 - e) * 2 + h
        return remote(
            state["sums"].at[e, h], state["extra"].at[5 - e, h], state["ps"].at[e * 2 + h], state["er"].at[slot], {"z": near}
        )

    def to_far(state, e, h):
        return remote(
            state["sums"].at[e, h], state["got"].at[1, h], state["ps"].at[e * 2 + h], state["gr"].at[2 + h],
            {"z": partner[e]},
        )

    def handover(state, e, h):
        return remote(
            state["part"].at[e, h, 1 - c], state["half"].at[e, h], state["hs"].at[e * 2 + h], state["hr"].at[e * 2 + h], to_c
        )

    def run(number, units_of, weights, factors, before, pick):
        state = stages[number]
        exit_k = weights.shape[0] - 1

        def step(i, carry):
            before(i)
            e = pick(i)
            s = partner_of(e)
            for h in range(2):
                beside(state, s, h).wait_recv()
            inputs = state["whole"][s].reshape(CORES * rows, features)
            hidden = units_of(inputs, weights, factors, taps_own[...])
            for h in range(2):
                last = weights[exit_k, :, :, pl.ds(h * half_width, half_width)].reshape(-1, half_width)
                total = jnp.dot(hidden, last, preferred_element_type=jnp.float32)
                state["part"][e, h] = total.astype(jnp.bfloat16).reshape(CORES, rows, half_width)
                handover(state, e, h).start()
            for h in range(2):
                handover(state, e, h).wait_recv()
                both = state["part"][e, h, c].astype(jnp.float32) + state["half"][e, h].astype(jnp.float32)
                state["sums"][e, h] = both.astype(jnp.bfloat16)

                @pl.when(e == 1)
                def _():
                    to_near(state, 1, h).start()

                @pl.when((1 - middle) * e > 1)
                def _():
                    to_merge(state, e, h).start()

            return carry

        lax.fori_loop(0, 4, step, 0)

        @pl.when(middle == 1)
        def _():
            for e in (2, 3) if number == 0 else (3, 2):
                for h in range(2):
                    far = state["extra"].at[e, h]
                    remote(far, far, state["ps"].at[e * 2 + h], state["er"].at[e * 2 + h], to_c).wait_recv()
                    both = state["sums"][e, h].astype(jnp.float32) + state["extra"][e, h].astype(jnp.float32)
                    state["sums"][e, h] = both.astype(jnp.bfloat16)
                    to_far(state, e, h).start()

    def finish(number, out, factor):
        state = stages[number]
        own = state["own"]
        gain_ref, shift_ref = norms[number]
        scale_row = 6 if number == 1 else 5
        pieces, one, two = [], 0.0, 0.0
        for h in range(2):
            cols = slice(h * half_width, (h + 1) * half_width)
            total = state["sums"][0, h].astype(jnp.float32)
            for k in range(2):
                src = state["got"].at[k, h]
                remote(src, src, state["ps"].at[h], state["gr"].at[k * 2 + h], to_c).wait_recv()
                total = total + state["got"][k, h].astype(jnp.float32)
            scale = lanes[scale_row : scale_row + 1, cols] * factor
            summed = RESIDUAL_SCALE * own[:, cols].astype(jnp.float32) + total * scale
            pieces.append(summed)
            one = one + jnp.sum(summed, -1, keepdims=True)
            two = two + jnp.sum(summed * summed, -1, keepdims=True)
        average = one / features
        variance = two / features - average * average
        inverse = lax.rsqrt(variance + EPSILON)
        for h in range(2):
            cols = slice(h * half_width, (h + 1) * half_width)
            normed = (pieces[h] - average) * inverse * gain_ref[:, cols] + shift_ref[:, cols]
            out[:, cols] = normed.astype(jnp.bfloat16)

    def mixer_arrivals(i):
        @pl.when(i > 0)
        def _():
            e = later_third(i)
            landed = m_place(x, partner_of(e), y)
            remote(landed, landed, mzsend.at[e], mzrecv.at[e], to_c).wait_recv()
            m_y(e).start()
            m_x(e).start()

    def line_arrivals(state):
        def before(i):
            @pl.when(i == 1)
            def _():
                for h in range(2):
                    pass_on(state, 1, h)

            @pl.when(i == 2)
            def _():
                pass_on(state, 2, 0)

            @pl.when(i == 2 + middle)
            def _():
                pass_on(state, 2, 1)

            @pl.when(i == 3)
            def _():
                for h in range(2):
                    pass_on(state, 3, h)

        return before

    run(
        0, feed_units, feed_w, units[:, : 2 * hidden_rows], mixer_arrivals,
        lambda i: (1 - middle) * (3 - i) + middle * lax.rem(i + 1, 4),
    )
    m_relay(0)
    m_relay(1)
    finish(0, own1, HALF_STEP)
    spread(stages[1], own1)
    m_relay(3)
    m_relay(2)
    for e in range(4):
        (m_x if e % 2 == 0 else m_y)(e).wait_recv()
        m_d(e).wait_recv()

    def arrival_order(i):
        return (1 - middle) * i + middle * ((i + 2) // 3) * (lax.rem(i + 1, 3) + 1)

    run(1, mixer_units, mixer_w, channels[...], line_arrivals(stages[1]), arrival_order)
    finish(1, own2, 1.0)
    spread(stages[2], own2)
    run(2, feed_units, feed_w, units[:, : 2 * hidden_rows], line_arrivals(stages[2]), arrival_order)
    finish(2, sheet, HALF_STEP)

    here = strip(place_here, rows)
    leaving = []
    for k, (tx, tc) in enumerate(((1 - x, c), (1 - x, 1 - c), (x, 1 - c))):
        there = strip(tx * CORES + tc, columns)
        leaving.append(
            remote(sheet.at[:, there], out_ref.at[here], fsend.at[k], frecv.at[k], {"x": tx, "c": tc})
        )
        leaving[-1].start()
    out_ref[here] = sheet[:, strip(place_here, columns)]

    for copy in trades + scale_sends + hops:
        copy.wait_send()
    for e, p in sent:
        y_copy(e, p).wait_send()
        x_copy(e, p).wait_send()
        d_copy(e, p).wait_send()
        if e > 0:
            z_copy(e, p).wait_send()
    for e in range(4):
        m_y(e).wait_send()
        m_x(e).wait_send()
        m_d(e).wait_send()
        if e > 0:
            m_z(e).wait_send()
    for state in stages:
        spread_done(state)
        for e in range(4):
            for h in range(2):
                handover(state, e, h).wait_send()
                if e > 0:
                    to_near(state, e, h).wait_send()
    for copy in leaving:
        copy.wait()


def column_plan(
    depth, tokens, gate_weight, up_weight, down_weight, gate_scale, up_scale, down_scale,
    bgate_weight, cgate_weight, value_weight, bgate_scale, cgate_scale, value_scale, conv_taps,
    mixout_weight, mixout_scale, first_gain, first_shift, mixer_gain, mixer_shift, last_gain, last_shift,
):
    dma = pltpu.SemaphoreType.DMA
    low, full = jnp.bfloat16, jnp.float32
    rows = tokens.shape[0] // (2 * CORES)
    features = tokens.shape[1] * 2 * CORES
    half_width = features // 2
    width = gate_weight.shape[0]
    hidden = gate_weight.shape[1]
    channels = bgate_weight.shape[1]
    lanes = max(-(-gate_scale.shape[1] // 128) * 128, 4 * bgate_scale.shape[1])
    big = [gate_weight, up_weight, down_weight, bgate_weight, cgate_weight, value_weight, mixout_weight]
    scales = [gate_scale, up_scale, bgate_scale, cgate_scale, value_scale, down_scale, mixout_scale]
    vectors = [first_gain, first_shift, mixer_gain, mixer_shift, last_gain, last_shift]
    operands = [tokens, *big, *scales, conv_taps] + [v[None] for v in vectors]
    scratch = [pltpu.VMEM(tokens.shape, low)] + [pltpu.VMEM(w.shape, full) for w in big]
    scratch += [
        pltpu.VMEM((3, hidden, width), low),
        pltpu.VMEM((4, channels, width), low),
        pltpu.VMEM((3, 2, hidden // depth, features), low),
        pltpu.VMEM((4, 2, channels // depth, features), low),
        pltpu.VMEM((8, lanes), full),
        pltpu.VMEM((CORES, 2, 2, depth, 8, lanes), full),
        pltpu.VMEM((8, features), full),
        pltpu.VMEM((8, -(-2 * hidden // depth // 128) * 128), full),
        pltpu.VMEM((8, 2 * channels // depth), full),
        pltpu.VMEM((TAPS, 2 * channels // depth), full),
    ]
    scratch += [pltpu.VMEM((rows, features), low) for _ in range(4)]
    for _ in range(3):
        scratch += [
            pltpu.VMEM((depth, CORES, rows, features), low),
            pltpu.VMEM((depth, 2, CORES, rows, half_width), low),
            pltpu.VMEM((depth, 2, rows, half_width), low),
            pltpu.VMEM((depth, 2, rows, half_width), low),
            pltpu.VMEM((depth, 2, rows, half_width), low),
            pltpu.VMEM((2, 2, rows, half_width), low),
        ]
    scratch += [dma((8,)), dma((3,)), dma((3,)), dma((6,)), dma((6,)), dma((3,)), dma((3,))]
    scratch += [dma((12,)) for _ in range(8)]
    scratch += [dma((4,)) for _ in range(8)]
    for _ in range(3):
        scratch += [dma((10,)) for _ in range(4)] + [dma((8,)) for _ in range(7)]
    return pl.pallas_call(
        layer_kernel,
        out_shape=jax.ShapeDtypeStruct(tokens.shape, low),
        in_specs=[ANY] * 8 + [VMEM] * (len(operands) - 8),
        out_specs=VMEM,
        scratch_shapes=scratch,
        compiler_params=pltpu.CompilerParams(
            collective_id=0, has_side_effects=True, vmem_limit_bytes=60 * 1024 * 1024
        ),
        name="layer",
    )(*operands)


def add_rows(gathered, shard_piece):
    return jnp.dot(gathered, shard_piece, preferred_element_type=jnp.float32)


def features(inputs):
    return lax.all_gather(inputs, "tp", axis=1, tiled=True)


def post_norm(residual, branch, norm_gain, norm_shift):
    summed = RESIDUAL_SCALE * residual.astype(jnp.float32) + branch
    moments = lax.psum((jnp.sum(summed, -1), jnp.sum(summed * summed, -1)), "tp")
    feature_total = summed.shape[1] * lax.axis_size("tp")
    average = (moments[0] / feature_total)[:, None]
    mean_square = (moments[1] / feature_total)[:, None]
    variance = mean_square - average * average
    return ((summed - average) * lax.rsqrt(variance + EPSILON) * norm_gain + norm_shift).astype(
        jnp.bfloat16
    )


def spread_back(weight_cols, left_rows):
    return (
        lax.psum_scatter(
            lax.dot_general(
                weight_cols, left_rows, (((0,), (1,)), ((), ())), preferred_element_type=jnp.float32
            ).astype(jnp.bfloat16),
            "tp",
            scatter_dimension=0,
            tiled=True,
        )
        .astype(jnp.float32)
        .T
    )


def shards(
    tokens,
    gate_weight,
    up_weight,
    down_weight,
    gate_scale,
    up_scale,
    down_scale,
    bgate_weight,
    cgate_weight,
    value_weight,
    bgate_scale,
    cgate_scale,
    value_scale,
    conv_taps,
    mixout_weight,
    mixout_scale,
    first_gain,
    first_shift,
    mixer_gain,
    mixer_shift,
    last_gain,
    last_shift,
):
    scales = (
        lax.all_gather(gate_scale, "fs", axis=1, tiled=True),
        lax.all_gather(up_scale, "fs", axis=1, tiled=True),
        lax.all_gather(down_scale, "fs", axis=1, tiled=True),
        lax.all_gather(bgate_scale, "fs", axis=1, tiled=True),
        lax.all_gather(cgate_scale, "fs", axis=1, tiled=True),
        lax.all_gather(value_scale, "fs", axis=1, tiled=True),
        lax.all_gather(mixout_scale, "fs", axis=1, tiled=True),
    )
    gate_cols, up_cols, down_cols, bgate_cols, cgate_cols, value_cols, mixout_cols = [
        scale_row.reshape(-1) for scale_row in scales
    ]
    tp_index = lax.axis_index("tp")
    columns = tokens.shape[1]

    def own_part(vector):
        return lax.dynamic_slice_in_dim(vector, tp_index * columns, columns)

    gate_low = gate_weight.astype(jnp.bfloat16)
    up_low = up_weight.astype(jnp.bfloat16)
    down_low = down_weight.astype(jnp.bfloat16)
    kept_gate, kept_up = (
        lax.all_gather(gate_low, "fs", axis=0, tiled=True),
        lax.all_gather(up_low, "fs", axis=0, tiled=True),
    )
    kept_down = lax.all_gather(down_low, "fs", axis=1, tiled=True)

    def channel_mix(gathered):
        gate_sum = jnp.dot(gathered, kept_gate, preferred_element_type=jnp.float32)
        up_sum = jnp.dot(gathered, kept_up, preferred_element_type=jnp.float32)
        hidden = (jax.nn.silu(gate_sum * gate_cols) * (up_sum * up_cols)).astype(jnp.bfloat16)
        return HALF_STEP * (spread_back(kept_down, hidden) * down_cols)

    first = post_norm(
        tokens, channel_mix(features(tokens)), own_part(first_gain), own_part(first_shift)
    )
    gathered = features(first)
    bgate_low = bgate_weight.astype(jnp.bfloat16)
    channels = bgate_low.shape[1]
    outgate = add_rows(gathered, lax.all_gather(bgate_low, "fs", axis=0, tiled=True))
    ingate = add_rows(
        gathered, lax.all_gather(cgate_weight.astype(jnp.bfloat16), "fs", axis=0, tiled=True)
    )
    values = add_rows(
        gathered, lax.all_gather(value_weight.astype(jnp.bfloat16), "fs", axis=0, tiled=True)
    )
    tap_weights = lax.dynamic_slice_in_dim(conv_taps, tp_index * channels, channels, 1)
    mixed = (ingate * cgate_cols * (values * value_cols)).reshape(-1, LENGTH, channels)
    padded = jnp.pad(mixed, ((0, 0), (TAPS - 1, 0), (0, 0)))
    convolved = jnp.zeros(mixed.shape, jnp.float32)
    for tap_index in range(TAPS):
        convolved = convolved + tap_weights[tap_index] * padded[:, tap_index : tap_index + LENGTH]
    gated = (outgate * bgate_cols * convolved.reshape(-1, channels)).astype(jnp.bfloat16)
    mix_full = lax.all_gather(mixout_weight.astype(jnp.bfloat16), "fs", axis=1, tiled=True)
    second = post_norm(
        first,
        spread_back(mix_full, gated) * mixout_cols,
        own_part(mixer_gain),
        own_part(mixer_shift),
    )
    return post_norm(
        second, channel_mix(features(second)), own_part(last_gain), own_part(last_shift)
    )


def solution(mesh):
    in_specs = (
        P("fs", "tp"),
        P("fs", "tp"),
        P("fs", "tp"),
        P("tp", "fs"),
        P("tp", "fs"),
        P("tp", "fs"),
        P("tp", "fs"),
        P("fs", "tp"),
        P("fs", "tp"),
        P("fs", "tp"),
        P("tp", "fs"),
        P("tp", "fs"),
        P("tp", "fs"),
        P(),
        P("tp", "fs"),
        P("tp", "fs"),
        P(),
        P(),
        P(),
        P(),
        P(),
        P(),
    )
    out_specs = P("fs", "tp")
    across = mesh.shape["tp"] // CORES
    if across == 2 and mesh.shape["fs"] == 8:
        depth = mesh.shape["fs"] // 2
        fine = Mesh(mesh.devices.reshape(depth, 2, 2, CORES), ("z", "y", "x", "c"))
        names = {"fs": ("z", "y"), "tp": ("x", "c")}

        def split(spec):
            return P(*(names.get(name) for name in spec))

        return jax.shard_map(
            functools.partial(column_plan, depth),
            mesh=fine,
            in_specs=tuple(split(spec) for spec in in_specs),
            out_specs=split(out_specs),
            check_vma=False,
        )
    return jax.shard_map(shards, mesh=mesh, in_specs=in_specs, out_specs=out_specs, check_vma=False)
```

time: 285 us -> 224 us (0.79)
  Pallas kernels: 261 us -> 222 us
  local copies, waits for them, and re-layouts: 11.4 us -> 1.67 us
  other arithmetic: 8 us -> 0 us
  starting transfers between devices: 4.38 us -> 0 us
    pallas_call x4 -> x1, Pallas kernels: 261 us -> 222 us  [column_plan(): pl.pallas_call(layer_kernel, out_shape=jax.ShapeDtypeStruct(tokens.shape,...]
    convert_element_type x7 -> x0, other arithmetic: 5.23 us -> none  [cut(): return matrix.astype(jnp.bfloat16).reshape(depth, -1, matrix.shape[1])]
    all_to_all x1 -> x0, starting transfers between devices: 4.38 us -> none  [column_plan(): own = lax.all_to_all(tokens, ('x', 'c'), 0, 1, tiled=True)]
    convert_element_type x5 -> x0, local copies, waits for them, and re-layouts: 3.1 us -> none  [cut(): return matrix.astype(jnp.bfloat16).reshape(depth, -1, matrix.shape[1])]
  transfers between devices with their start and end apart: 1 -> 0, of which waited for: 0 -> 0; matrix products, arithmetic and copies ran while one was open for 5% -> 0% of each run, Pallas kernels for 0% -> 0%
where the time goes in v2:
time: 224 us
  Pallas kernels  222 us (99%)
    pallas_call x1, Pallas kernels, column_plan(): pl.pallas_call(layer_kernel, out_shape=jax.ShapeDtypeStruct(tokens.shape,...  222 us

profile of v2, /device:TPU:1, one launch (start us, length us, event | category | flops | bytes accessed | tf_op | source)
XLA Modules:
  0.0 223.8 jit_solution(16815855691312896397)
XLA Ops:
  0.0 222.1 %layer.1 = bf16[256,512]{1,0:T(8,128)(2,1)} custom-call(bf16[256,512]{1,0:T(8,128)(2,1)} %tokens_ref.1, f32[256,1408]{1,0:T(8,128)} %gate_ref.1, f32[256,1408]{1,0:T(8,128)} %up_ref.1, f32[1408,256]{1,0:T(8,128)} %down_ref.1, f32[256,512]{1,0:T(8,128)} %b_ref.1, f32[256,512]{1,0:T(8,128)} %c_ref.1, f32[256,512]{1,0:T(8,128)} %v_ref.1, f32[512,256]{1,0:T(8,128)} %mix_ref.1, ...), custom_call_target="tpu_custom_call" | custom-call | tf_op jit(solution)/shard_map/layer/pallas_call | solution.py:593
  222.1 1.7 copy.24

commit v3 on v2

--- a/solution.py
+++ b/solution.py
@@ -110,6 +110,12 @@
         pack[k : k + 1, 0 : scale_ref.shape[1]] = scale_ref[...]
     pl.semaphore_wait(barrier, len(greeted))
 
+    scale_sends = []
+    for e in (1, 2, 3):
+        scale_sends.append(remote(pack, blocks.at[c, x, y, z], ssend.at[e], srecv.at[e], {"z": partner[e]}))
+        scale_sends[-1].start()
+    blocks[c, x, y, z] = pack[...]
+
     rows, features = own0.shape
     columns = tin.shape[1]
     place_here = x * CORES + c
@@ -188,12 +194,6 @@
             z_copy(e, p).start()
     for p in order:
         feed_w[p, x, :, strip(z * 2 + y, width)] = wsend[p, strip(z, hidden_rows)]
-
-    scale_sends = []
-    for e in (1, 2, 3):
-        scale_sends.append(remote(pack, blocks.at[c, x, y, z], ssend.at[e], srecv.at[e], {"z": partner[e]}))
-        scale_sends[-1].start()
-    blocks[c, x, y, z] = pack[...]
 
     def piece(state, s, h):
         return state["whole"].at[s, c, pl.ds(h * (rows // 2), rows // 2)]
@@ -473,11 +473,8 @@
 
             @pl.when(i == 2)
             def _():
-                pass_on(state, 2, 0)
-
-            @pl.when(i == 2 + middle)
-            def _():
-                pass_on(state, 2, 1)
+                for h in range(2):
+                    pass_on(state, 2, h)
 
             @pl.when(i == 3)
             def _():

time: 224 us -> 196 us (0.88)
  Pallas kernels: 222 us -> 194 us
    pallas_call x1, Pallas kernels: 222 us -> 194 us  [column_plan(): pl.pallas_call(layer_kernel, out_shape=jax.ShapeDtypeStruct(tokens.shape,...]
where the time goes in v3:
time: 196 us; the launch traced here: 195 us
  Pallas kernels  194 us (99%)
    pallas_call x1, Pallas kernels, column_plan(): pl.pallas_call(layer_kernel, out_shape=jax.ShapeDtypeStruct(tokens.shape,...  194 us

profile of v3, /device:TPU:1, one launch (start us, length us, event | category | flops | bytes accessed | tf_op | source)
XLA Modules:
  0.0 195.5 jit_solution(3148944225662413914)
XLA Ops:
  0.0 193.8 %layer.1 = bf16[256,512]{1,0:T(8,128)(2,1)} custom-call(bf16[256,512]{1,0:T(8,128)(2,1)} %tokens_ref.1, f32[256,1408]{1,0:T(8,128)} %gate_ref.1, f32[256,1408]{1,0:T(8,128)} %up_ref.1, f32[1408,256]{1,0:T(8,128)} %down_ref.1, f32[256,512]{1,0:T(8,128)} %b_ref.1, f32[256,512]{1,0:T(8,128)} %c_ref.1, f32[256,512]{1,0:T(8,128)} %v_ref.1, f32[512,256]{1,0:T(8,128)} %mix_ref.1, ...), custom_call_target="tpu_custom_call" | custom-call | tf_op jit(solution)/shard_map/layer/pallas_call | solution.py:590
  193.8 1.7 copy.24

commit v4 on v3

--- a/solution.py
+++ b/solution.py
@@ -11,12 +11,14 @@
 TAPS = 3
 LENGTH = 128
 CORES = 2
+ROW_CUTS = 2
+COLUMN_CUTS = 2
 
 RESIDUAL_SCALE = 1.4142135623730951
 HALF_STEP = 0.5
 EPSILON = 1e-05
 BY_AXIS = pl.DeviceIdType.MESH
-ANY = pl.BlockSpec(memory_space=pl.ANY)
+HBM = pl.BlockSpec(memory_space=pltpu.HBM)
 VMEM = pl.BlockSpec(memory_space=pltpu.VMEM)
 
 
@@ -63,10 +65,11 @@
 ):
     refs = list(refs)
     take = lambda n: [refs.pop(0) for _ in range(n)]
-    scale_refs = take(7)
-    taps_ref = take(1)[0]
-    norms = [take(2) for _ in range(3)]
+    small = take(14)
     (out_ref,) = take(1)
+    held = take(14)
+    scale_refs, taps_ref = held[:7], held[7]
+    norms = [held[8 + 2 * k : 10 + 2 * k] for k in range(3)]
     tin, gate_full, up_full, down_full, *mixer_full = take(8)
     wsend, msend, feed_w, mixer_w, pack, blocks, lanes, units, channels, taps_own = take(10)
     own0, own1, own2, sheet = take(4)
@@ -99,7 +102,8 @@
             )
         )
     ]
-    for load in loads:
+    little = [pltpu.make_async_copy(src, dst, local.at[8 + k]) for k, (src, dst) in enumerate(zip(small, held))]
+    for load in little[:7] + loads + little[7:]:
         load.start()
     barrier = pltpu.get_barrier_semaphore()
     greeted = [{"z": t} for t in partner[1:]] + [to_x, to_y, to_c, {"x": 1 - x, "c": 1 - c}]
@@ -107,6 +111,7 @@
         pl.semaphore_signal(barrier, inc=1, device_id=target, device_id_type=BY_AXIS)
     pack[...] = jnp.zeros_like(pack)
     for k, scale_ref in enumerate(scale_refs):
+        little[k].wait()
         pack[k : k + 1, 0 : scale_ref.shape[1]] = scale_ref[...]
     pl.semaphore_wait(barrier, len(greeted))
 
@@ -195,33 +200,48 @@
     for p in order:
         feed_w[p, x, :, strip(z * 2 + y, width)] = wsend[p, strip(z, hidden_rows)]
 
+    cut_rows = rows // ROW_CUTS
+
     def piece(state, s, h):
-        return state["whole"].at[s, c, pl.ds(h * (rows // 2), rows // 2)]
+        return state["whole"].at[s, c, pl.ds(h * cut_rows, cut_rows)]
+
+    def beside(state, s, h, src=None):
+        dst = piece(state, s, h)
+        slot = s * ROW_CUTS + h
+        return remote(dst if src is None else src, dst, state["cs"].at[slot], state["cr"].at[slot], to_c)
+
+    def rightward(state, s, k, h, src=None):
+        dst = piece(state, s, h)
+        slot = k * ROW_CUTS + h
+        return remote(
+            dst if src is None else src, dst, state["rs"].at[slot], state["rr"].at[slot + ROW_CUTS], {"z": z + 1}
+        )
+
+    def leftward(state, s, k, h, src=None):
+        dst = piece(state, s, h)
+        slot = k * ROW_CUTS + h
+        return remote(
+            dst if src is None else src, dst, state["ls"].at[slot], state["lr"].at[slot + ROW_CUTS], {"z": z - 1}
+        )
 
     def spread(state, own):
         state["own"] = own
-        for h in range(2):
-            src = own.at[pl.ds(h * (rows // 2), rows // 2)]
+        for h in range(ROW_CUTS):
+            src = own.at[pl.ds(h * cut_rows, cut_rows)]
 
             @pl.when(z < 3)
             def _():
-                remote(src, piece(state, z, h), state["rs"].at[h], state["rr"].at[2 + h], {"z": z + 1}).start()
+                rightward(state, z, 0, h, src).start()
 
             @pl.when(z > 0)
             def _():
-                remote(src, piece(state, z, h), state["ls"].at[h], state["lr"].at[2 + h], {"z": z - 1}).start()
-
-        for h in range(2):
-            src = own.at[pl.ds(h * (rows // 2), rows // 2)]
-            remote(src, piece(state, z, h), state["cs"].at[z * 2 + h], state["cr"].at[z * 2 + h], to_c).start()
+                leftward(state, z, 0, h, src).start()
+
+            beside(state, z, h, src).start()
         state["whole"][z, c] = own[...]
 
-    def beside(state, s, h):
-        src = piece(state, s, h)
-        return remote(src, src, state["cs"].at[s * 2 + h], state["cr"].at[s * 2 + h], to_c)
-
     def pass_on(state, k, h):
-        slot = k * 2 + h
+        slot = k * ROW_CUTS + h
 
         @pl.when(z >= k)
         def _():
@@ -231,7 +251,7 @@
 
             @pl.when(z < 3)
             def _():
-                remote(src, src, state["rs"].at[slot], state["rr"].at[slot + 2], {"z": z + 1}).start()
+                rightward(state, s, k, h).start()
 
             beside(state, s, h).start()
 
@@ -243,23 +263,21 @@
 
             @pl.when(z > 0)
             def _():
-                remote(src, src, state["ls"].at[slot], state["lr"].at[slot + 2], {"z": z - 1}).start()
+                leftward(state, s, k, h).start()
 
             beside(state, s, h).start()
 
     def spread_done(state):
         for k in range(4):
-            for h in range(2):
-                slot = k * 2 + h
-                src = piece(state, z, h)
+            for h in range(ROW_CUTS):
 
                 @pl.when((z >= k) & (z < 3))
                 def _():
-                    remote(src, src, state["rs"].at[slot], state["rr"].at[slot], to_c).wait_send()
+                    rightward(state, z, k, h).wait_send()
 
                 @pl.when((z + k < 4) & (z > 0))
                 def _():
-                    remote(src, src, state["ls"].at[slot], state["lr"].at[slot], to_c).wait_send()
+                    leftward(state, z, k, h).wait_send()
 
                 beside(state, k, h).wait_send()
 
@@ -289,15 +307,18 @@
         return remote(src, m_place(x, z, y), mzsend.at[e], mzrecv.at[e], {"z": partner_of(e)})
 
     def m_d(e):
-        if e % 2 == 0:
-            block = m_place(x, partner[e], 1 - y)
-            return remote(block, block, mdsend.at[e], mdrecv.at[e], to_x)
-        block = m_place(1 - x, partner[e], y)
-        return remote(block, block, mdsend.at[e], mdrecv.at[e], to_y)
+        mats = mixer_w.shape[0] // 2
+        over_y = m_place(x, partner[e], 1 - y).at[pl.ds(0, mats)]
+        over_x = m_place(1 - x, partner[e], y).at[pl.ds(mats, mats)]
+        return (
+            remote(over_y, over_y, mdsend.at[2 * e], mdrecv.at[2 * e], to_x),
+            remote(over_x, over_x, mdsend.at[2 * e + 1], mdrecv.at[2 * e + 1], to_y),
+        )
 
     def m_relay(e):
-        (m_y if e % 2 == 0 else m_x)(e).wait_recv()
-        m_d(e).start()
+        for arrival, copy in zip((m_y, m_x), m_d(e)):
+            arrival(e).wait_recv()
+            copy.start()
 
     hops = [
         remote(part, part, ssend.at[slot], srecv.at[slot], target)
@@ -321,7 +342,7 @@
             hops[j // 2 - 2].wait_recv()
             hops[j // 2 - 1].start()
     for k in range(1, 4):
-        for h in range(2):
+        for h in range(ROW_CUTS):
             pass_on(stages[0], k, h)
     for e in (1, 3, 2):
         m_z(e).start()
@@ -350,6 +371,8 @@
                 low, high = (blocks[pc, px, py, pz][:, 0:pair] for py in range(2))
                 start = ((px * CORES + pc) * 4 + pz) * pair
                 lanes[:, start : start + pair] = low + pltpu.roll(high, lane_part, 1)
+    for load in little[7:]:
+        load.wait()
     for px in range(2):
         taps_own[:, px * pair : (px + 1) * pair] = taps_ref[:, strip((px * CORES + c) * 4 + z, pair)]
 
@@ -361,28 +384,32 @@
         (x_copy if (e + p) % 2 == 0 else y_copy)(e, p).wait_recv()
         d_copy(e, p).wait_recv()
 
-    half_width = features // 2
+    cut_width = features // COLUMN_CUTS
+    cuts = range(COLUMN_CUTS)
 
     def to_near(state, e, h):
         return remote(
-            state["sums"].at[e, h], state["got"].at[0, h], state["ps"].at[e * 2 + h], state["gr"].at[h], {"z": near}
+            state["sums"].at[e, h], state["got"].at[0, h], state["ps"].at[e * COLUMN_CUTS + h], state["gr"].at[h],
+            {"z": near},
         )
 
     def to_merge(state, e, h):
-        slot = (5 - e) * 2 + h
+        slot = (5 - e) * COLUMN_CUTS + h
         return remote(
-            state["sums"].at[e, h], state["extra"].at[5 - e, h], state["ps"].at[e * 2 + h], state["er"].at[slot], {"z": near}
+            state["sums"].at[e, h], state["extra"].at[5 - e, h], state["ps"].at[e * COLUMN_CUTS + h],
+            state["er"].at[slot], {"z": near},
         )
 
     def to_far(state, e, h):
         return remote(
-            state["sums"].at[e, h], state["got"].at[1, h], state["ps"].at[e * 2 + h], state["gr"].at[2 + h],
-            {"z": partner[e]},
+            state["sums"].at[e, h], state["got"].at[1, h], state["ps"].at[e * COLUMN_CUTS + h],
+            state["gr"].at[COLUMN_CUTS + h], {"z": partner[e]},
         )
 
     def handover(state, e, h):
+        slot = e * COLUMN_CUTS + h
         return remote(
-            state["part"].at[e, h, 1 - c], state["half"].at[e, h], state["hs"].at[e * 2 + h], state["hr"].at[e * 2 + h], to_c
+            state["part"].at[e, h, 1 - c], state["half"].at[e, h], state["hs"].at[slot], state["hr"].at[slot], to_c
         )
 
     def run(number, units_of, weights, factors, before, pick):
@@ -393,16 +420,16 @@
             before(i)
             e = pick(i)
             s = partner_of(e)
-            for h in range(2):
+            for h in range(ROW_CUTS):
                 beside(state, s, h).wait_recv()
             inputs = state["whole"][s].reshape(CORES * rows, features)
             hidden = units_of(inputs, weights, factors, taps_own[...])
-            for h in range(2):
-                last = weights[exit_k, :, :, pl.ds(h * half_width, half_width)].reshape(-1, half_width)
+            for h in cuts:
+                last = weights[exit_k, :, :, pl.ds(h * cut_width, cut_width)].reshape(-1, cut_width)
                 total = jnp.dot(hidden, last, preferred_element_type=jnp.float32)
-                state["part"][e, h] = total.astype(jnp.bfloat16).reshape(CORES, rows, half_width)
+                state["part"][e, h] = total.astype(jnp.bfloat16).reshape(CORES, rows, cut_width)
                 handover(state, e, h).start()
-            for h in range(2):
+            for h in cuts:
                 handover(state, e, h).wait_recv()
                 both = state["part"][e, h, c].astype(jnp.float32) + state["half"][e, h].astype(jnp.float32)
                 state["sums"][e, h] = both.astype(jnp.bfloat16)
@@ -422,9 +449,9 @@
         @pl.when(middle == 1)
         def _():
             for e in (2, 3) if number == 0 else (3, 2):
-                for h in range(2):
+                for h in cuts:
                     far = state["extra"].at[e, h]
-                    remote(far, far, state["ps"].at[e * 2 + h], state["er"].at[e * 2 + h], to_c).wait_recv()
+                    remote(far, far, state["ps"].at[h], state["er"].at[e * COLUMN_CUTS + h], to_c).wait_recv()
                     both = state["sums"][e, h].astype(jnp.float32) + state["extra"][e, h].astype(jnp.float32)
                     state["sums"][e, h] = both.astype(jnp.bfloat16)
                     to_far(state, e, h).start()
@@ -435,12 +462,12 @@
         gain_ref, shift_ref = norms[number]
         scale_row = 6 if number == 1 else 5
         pieces, one, two = [], 0.0, 0.0
-        for h in range(2):
-            cols = slice(h * half_width, (h + 1) * half_width)
+        for h in cuts:
+            cols = slice(h * cut_width, (h + 1) * cut_width)
             total = state["sums"][0, h].astype(jnp.float32)
             for k in range(2):
                 src = state["got"].at[k, h]
-                remote(src, src, state["ps"].at[h], state["gr"].at[k * 2 + h], to_c).wait_recv()
+                remote(src, src, state["ps"].at[h], state["gr"].at[k * COLUMN_CUTS + h], to_c).wait_recv()
                 total = total + state["got"][k, h].astype(jnp.float32)
             scale = lanes[scale_row : scale_row + 1, cols] * factor
             summed = RESIDUAL_SCALE * own[:, cols].astype(jnp.float32) + total * scale
@@ -450,8 +477,8 @@
         average = one / features
         variance = two / features - average * average
         inverse = lax.rsqrt(variance + EPSILON)
-        for h in range(2):
-            cols = slice(h * half_width, (h + 1) * half_width)
+        for h in cuts:
+            cols = slice(h * cut_width, (h + 1) * cut_width)
             normed = (pieces[h] - average) * inverse * gain_ref[:, cols] + shift_ref[:, cols]
             out[:, cols] = normed.astype(jnp.bfloat16)
 
@@ -464,24 +491,21 @@
             m_y(e).start()
             m_x(e).start()
 
-    def line_arrivals(state):
-        def before(i):
-            @pl.when(i == 1)
-            def _():
-                for h in range(2):
-                    pass_on(state, 1, h)
-
-            @pl.when(i == 2)
-            def _():
-                for h in range(2):
-                    pass_on(state, 2, h)
-
-            @pl.when(i == 3)
-            def _():
-                for h in range(2):
-                    pass_on(state, 3, h)
-
-        return before
+    def arrival_order(i):
+        return (1 - middle) * i + middle * ((i + 2) // 3) * (lax.rem(i + 1, 3) + 1)
+
+    def pass_all(state, k):
+        for h in range(ROW_CUTS):
+            pass_on(state, k, h)
+
+    def arrivals_second(i):
+        pl.when((i == 1) & (middle == 0))(lambda: pass_all(stages[1], 2))
+        pl.when(i == 2)(lambda: pass_all(stages[1], 3))
+
+    def arrivals_third(i):
+        pl.when(i == 1)(lambda: pass_all(stages[2], 1))
+        pl.when(i == 2 - middle)(lambda: pass_all(stages[2], 2))
+        pl.when(i == 3)(lambda: pass_all(stages[2], 3))
 
     run(
         0, feed_units, feed_w, units[:, : 2 * hidden_rows], mixer_arrivals,
@@ -489,21 +513,23 @@
     )
     m_relay(0)
     m_relay(1)
+    m_relay(3)
     finish(0, own1, HALF_STEP)
     spread(stages[1], own1)
-    m_relay(3)
+    pl.when(middle == 1)(lambda: pass_all(stages[1], 1))
     m_relay(2)
+    pl.when(middle == 0)(lambda: pass_all(stages[1], 1))
+    pl.when(middle == 1)(lambda: pass_all(stages[1], 2))
     for e in range(4):
-        (m_x if e % 2 == 0 else m_y)(e).wait_recv()
-        m_d(e).wait_recv()
-
-    def arrival_order(i):
-        return (1 - middle) * i + middle * ((i + 2) // 3) * (lax.rem(i + 1, 3) + 1)
-
-    run(1, mixer_units, mixer_w, channels[...], line_arrivals(stages[1]), arrival_order)
+        for copy in m_d(e):
+            copy.wait_recv()
+    run(
+        1, mixer_units, mixer_w, channels[...], arrivals_second,
+        lambda i: arrival_order(lax.rem(i + 1, 4)),
+    )
     finish(1, own2, 1.0)
     spread(stages[2], own2)
-    run(2, feed_units, feed_w, units[:, : 2 * hidden_rows], line_arrivals(stages[2]), arrival_order)
+    run(2, feed_units, feed_w, units[:, : 2 * hidden_rows], arrivals_third, arrival_order)
     finish(2, sheet, HALF_STEP)
 
     here = strip(place_here, rows)
@@ -527,13 +553,14 @@
     for e in range(4):
         m_y(e).wait_send()
         m_x(e).wait_send()
-        m_d(e).wait_send()
+        for copy in m_d(e):
+            copy.wait_send()
         if e > 0:
             m_z(e).wait_send()
     for state in stages:
         spread_done(state)
         for e in range(4):
-            for h in range(2):
+            for h in cuts:
                 handover(state, e, h).wait_send()
                 if e > 0:
                     to_near(state, e, h).wait_send()
@@ -550,7 +577,7 @@
     low, full = jnp.bfloat16, jnp.float32
     rows = tokens.shape[0] // (2 * CORES)
     features = tokens.shape[1] * 2 * CORES
-    half_width = features // 2
+    cut_width = features // COLUMN_CUTS
     width = gate_weight.shape[0]
     hidden = gate_weight.shape[1]
     channels = bgate_weight.shape[1]
@@ -559,7 +586,8 @@
     scales = [gate_scale, up_scale, bgate_scale, cgate_scale, value_scale, down_scale, mixout_scale]
     vectors = [first_gain, first_shift, mixer_gain, mixer_shift, last_gain, last_shift]
     operands = [tokens, *big, *scales, conv_taps] + [v[None] for v in vectors]
-    scratch = [pltpu.VMEM(tokens.shape, low)] + [pltpu.VMEM(w.shape, full) for w in big]
+    scratch = [pltpu.VMEM(operand.shape, full) for operand in operands[8:]]
+    scratch += [pltpu.VMEM(tokens.shape, low)] + [pltpu.VMEM(w.shape, full) for w in big]
     scratch += [
         pltpu.VMEM((3, hidden, width), low),
         pltpu.VMEM((4, channels, width), low),
@@ -576,21 +604,21 @@
     for _ in range(3):
         scratch += [
             pltpu.VMEM((depth, CORES, rows, features), low),
-            pltpu.VMEM((depth, 2, CORES, rows, half_width), low),
-            pltpu.VMEM((depth, 2, rows, half_width), low),
-            pltpu.VMEM((depth, 2, rows, half_width), low),
-            pltpu.VMEM((depth, 2, rows, half_width), low),
-            pltpu.VMEM((2, 2, rows, half_width), low),
+            pltpu.VMEM((depth, COLUMN_CUTS, CORES, rows, cut_width), low),
+            pltpu.VMEM((depth, COLUMN_CUTS, rows, cut_width), low),
+            pltpu.VMEM((depth, COLUMN_CUTS, rows, cut_width), low),
+            pltpu.VMEM((depth, COLUMN_CUTS, rows, cut_width), low),
+            pltpu.VMEM((2, COLUMN_CUTS, rows, cut_width), low),
         ]
-    scratch += [dma((8,)), dma((3,)), dma((3,)), dma((6,)), dma((6,)), dma((3,)), dma((3,))]
+    scratch += [dma((len(operands),)), dma((3,)), dma((3,)), dma((6,)), dma((6,)), dma((3,)), dma((3,))]
     scratch += [dma((12,)) for _ in range(8)]
-    scratch += [dma((4,)) for _ in range(8)]
+    scratch += [dma((4,)) for _ in range(6)] + [dma((8,)) for _ in range(2)]
     for _ in range(3):
-        scratch += [dma((10,)) for _ in range(4)] + [dma((8,)) for _ in range(7)]
+        scratch += [dma((5 * ROW_CUTS,)) for _ in range(6)] + [dma((4 * COLUMN_CUTS,)) for _ in range(5)]
     return pl.pallas_call(
         layer_kernel,
         out_shape=jax.ShapeDtypeStruct(tokens.shape, low),
-        in_specs=[ANY] * 8 + [VMEM] * (len(operands) - 8),
+        in_specs=[HBM] * len(operands),
         out_specs=VMEM,
         scratch_shapes=scratch,
         compiler_params=pltpu.CompilerParams(

time: 196 us -> 193 us (0.985)
  Pallas kernels: 194 us -> 191 us
    pallas_call x1, Pallas kernels: 194 us -> 191 us  [column_plan(): pl.pallas_call(layer_kernel, out_shape=jax.ShapeDtypeStruct(tokens.shape,...]
where the time goes in v4:
time: 193 us
  Pallas kernels  191 us (99%)
    pallas_call x1, Pallas kernels, column_plan(): pl.pallas_call(layer_kernel, out_shape=jax.ShapeDtypeStruct(tokens.shape,...  191 us

profile of v4, /device:TPU:1, one launch (start us, length us, event | category | flops | bytes accessed | tf_op | source)
XLA Modules:
  0.0 192.5 jit_solution(781947826174083890)
XLA Ops:
  0.0 190.9 %layer.1 = bf16[256,512]{1,0:T(8,128)(2,1)} custom-call(bf16[256,512]{1,0:T(8,128)(2,1)} %tokens_ref.1, f32[256,1408]{1,0:T(8,128)} %gate_ref.1, f32[256,1408]{1,0:T(8,128)} %up_ref.1, f32[1408,256]{1,0:T(8,128)} %down_ref.1, f32[256,512]{1,0:T(8,128)} %b_ref.1, f32[256,512]{1,0:T(8,128)} %c_ref.1, f32[256,512]{1,0:T(8,128)} %v_ref.1, f32[512,256]{1,0:T(8,128)} %mix_ref.1, ...), custom_call_target="tpu_custom_call" | custom-call | tf_op jit(solution)/shard_map/layer/pallas_call | solution.py:618
  190.9 1.7 copy.24

commit v5 on v4

--- a/solution.py
+++ b/solution.py
@@ -240,7 +240,7 @@
             beside(state, z, h, src).start()
         state["whole"][z, c] = own[...]
 
-    def pass_on(state, k, h):
+    def pass_right(state, k, h):
         slot = k * ROW_CUTS + h
 
         @pl.when(z >= k)
@@ -255,6 +255,9 @@
 
             beside(state, s, h).start()
 
+    def pass_left(state, k, h):
+        slot = k * ROW_CUTS + h
+
         @pl.when(z + k < 4)
         def _():
             s = lax.rem(z + k, 4)
@@ -266,6 +269,20 @@
                 leftward(state, s, k, h).start()
 
             beside(state, s, h).start()
+
+    def sooner(state, k):
+        for h in range(ROW_CUTS):
+            pl.when(z < 2)(lambda: pass_left(state, k, h))
+            pl.when(z >= 2)(lambda: pass_right(state, k, h))
+
+    def later(state, k):
+        for h in range(ROW_CUTS):
+            pl.when(z < 2)(lambda: pass_right(state, k, h))
+            pl.when(z >= 2)(lambda: pass_left(state, k, h))
+
+    def pass_all(state, k):
+        sooner(state, k)
+        later(state, k)
 
     def spread_done(state):
         for k in range(4):
@@ -343,7 +360,8 @@
             hops[j // 2 - 1].start()
     for k in range(1, 4):
         for h in range(ROW_CUTS):
-            pass_on(stages[0], k, h)
+            pass_right(stages[0], k, h)
+            pass_left(stages[0], k, h)
     for e in (1, 3, 2):
         m_z(e).start()
     mine = msend.at[:, strip(z, channel_rows)]
@@ -493,10 +511,6 @@
 
     def arrival_order(i):
         return (1 - middle) * i + middle * ((i + 2) // 3) * (lax.rem(i + 1, 3) + 1)
-
-    def pass_all(state, k):
-        for h in range(ROW_CUTS):
-            pass_on(state, k, h)
 
     def arrivals_second(i):
         pl.when((i == 1) & (middle == 0))(lambda: pass_all(stages[1], 2))

time: 193 us -> 192 us (level)
  no operation moved by 1% of the time
where the time goes in v5:
time: 192 us
  Pallas kernels  190 us (99%)
    pallas_call x1, Pallas kernels, column_plan(): pl.pallas_call(layer_kernel, out_shape=jax.ShapeDtypeStruct(tokens.shape,...  190 us

profile of v5, /device:TPU:1, one launch (start us, length us, event | category | flops | bytes accessed | tf_op | source)
XLA Modules:
  0.0 192.1 jit_solution(16855609907190648011)
XLA Ops:
  0.0 190.4 %layer.1 = bf16[256,512]{1,0:T(8,128)(2,1)} custom-call(bf16[256,512]{1,0:T(8,128)(2,1)} %tokens_ref.1, f32[256,1408]{1,0:T(8,128)} %gate_ref.1, f32[256,1408]{1,0:T(8,128)} %up_ref.1, f32[1408,256]{1,0:T(8,128)} %down_ref.1, f32[256,512]{1,0:T(8,128)} %b_ref.1, f32[256,512]{1,0:T(8,128)} %c_ref.1, f32[256,512]{1,0:T(8,128)} %v_ref.1, f32[512,256]{1,0:T(8,128)} %mix_ref.1, ...), custom_call_target="tpu_custom_call" | custom-call | tf_op jit(solution)/shard_map/layer/pallas_call | solution.py:632
  190.4 1.7 copy.24
